TPU v7x, 512 devices: a whole 4x4x16 slice. The times are simulated.
512 devices in a mesh: sp: 16 (over z), dp: 32 (over y, x, core).
Axes of the slice: x: 4, y: 4, z: 16, core: 2. Of those that a mesh axis runs over, the one named last changes fastest.
Arguments:
- tokens: bfloat16 [32, 2048, 2048], P('dp', 'sp'), may hold values from -6 to 6
- receptance_weight: bfloat16 [2048, 1024], P('dp'), may hold values from -0.125 to 0.125
- key_projection_weight: bfloat16 [2048, 1024], P('dp'), may hold values from -0.125 to 0.125
- value_projection_weight: bfloat16 [2048, 1024], P('dp'), may hold values from -0.125 to 0.125
- decay_down_weight: bfloat16 [2048, 256], P('dp'), may hold values from -0.125 to 0.125
- decay_up_weight: bfloat16 [2, 128, 1024], replicated, may hold values from -0.71875 to 0.71875
- decay_floor_level: float32 [2, 1024], replicated, may hold values from -10 to -2.25
- correction_rate_logit: float32 [2, 1024], P(None, 'sp'), may hold values from -4 to 4
- diagonal_address_factor: float32 [2, 1024], P(None, 'sp'), may hold values from -1 to 1
- head_norm_gain: float32 [1024], P('sp'), may hold values from 0.1 to 1.9
Outputs:
- mixed: bfloat16 [32, 2048, 1024], P('dp', 'sp')
All inputs are finite; a program needn't handle non-finite values.
Results may differ from a plain program's by a relative error of at most 0.0056.
The roundings to bfloat16 on the way count: a program that leaves them out, or rounds other values in their place, can miss the bound.
Values may be sent and summed in bfloat16 or wider, within the bound.
No kernel may reach another device: no remote copies, remote signals or barrier semaphores. Data moves between devices by JAX's collectives and lax.ppermute only.
A program may use at most 128 MiB of HBM per device.

v0:
```python
import math

import jax
import jax.numpy as jnp
from jax import lax
from jax.sharding import PartitionSpec as P

SUBSPACE_SIZE = 64


def in_one_piece(arrays, axis, dim, along):
    both = jnp.concatenate(arrays, axis=along)
    result, at, outs = (lax.all_gather(both, axis, axis=dim, tiled=True), 0, [])
    for a in arrays:
        outs.append(lax.slice_in_dim(result, at, at + a.shape[along], axis=along))
        at += a.shape[along]
    return tuple(outs)


def contract(pattern, former, latter):
    return jnp.einsum(pattern, former, latter, precision=lax.Precision.HIGHEST)


def project_rows(totals, pieces, source):
    results = []
    for running, piece in zip(totals, pieces):
        results.append(jnp.dot(source, piece, preferred_element_type=jnp.float32))
    return tuple(results)


def both_ways(content_matrix_full):
    return jnp.stack([content_matrix_full, jnp.flip(content_matrix_full, 0)], 0)


def advance(state, pair):
    transfer_block, inject_block = pair
    later = contract("...ij,...jk->...ik", state, transfer_block) + inject_block
    return (later, state)


def per_device(
    tokens,
    receptance_weight,
    key_projection_weight,
    value_projection_weight,
    decay_down_weight,
    decay_up_weight,
    decay_floor_level,
    correction_rate_logit,
    diagonal_address_factor,
    head_norm_gain,
):
    depth = tokens.shape[2]
    source = tokens.reshape(-1, depth)
    row_count = source.shape[0]
    channels = receptance_weight.shape[1]
    low_width = decay_down_weight.shape[1]
    empty = jnp.zeros((row_count, channels), jnp.float32)
    initial = (empty, empty, empty, jnp.zeros((row_count, low_width), jnp.float32))
    sums = project_rows(
        initial,
        in_one_piece(
            (receptance_weight, key_projection_weight, value_projection_weight, decay_down_weight),
            "dp",
            0,
            1,
        ),
        source,
    )
    receive = sums[0].astype(jnp.bfloat16)
    key_rows = sums[1].astype(jnp.bfloat16)
    value_rows = sums[2].astype(jnp.bfloat16)
    lowered = jnp.tanh(sums[3]).astype(jnp.bfloat16)
    rank = decay_up_weight.shape[1]
    forward_pre = (
        jnp.dot(lowered[:, :rank], decay_up_weight[0], preferred_element_type=jnp.float32)
        + decay_floor_level[0]
    ).astype(jnp.bfloat16)
    backward_pre = (
        jnp.dot(lowered[:, rank:], decay_up_weight[1], preferred_element_type=jnp.float32)
        + decay_floor_level[1]
    ).astype(jnp.bfloat16)
    moved = (
        lax.all_to_all(receive, "sp", split_axis=1, concat_axis=0, tiled=True),
        lax.all_to_all(key_rows, "sp", split_axis=1, concat_axis=0, tiled=True),
        lax.all_to_all(value_rows, "sp", split_axis=1, concat_axis=0, tiled=True),
        lax.all_to_all(forward_pre, "sp", split_axis=1, concat_axis=0, tiled=True),
        lax.all_to_all(backward_pre, "sp", split_axis=1, concat_axis=0, tiled=True),
    )
    length = moved[0].shape[0]
    local_channels = moved[0].shape[1]
    subspace_dimension = SUBSPACE_SIZE
    subspace_batches = local_channels // subspace_dimension
    span = math.gcd(length, 64)
    blocks = length // span

    def by_head(content_matrix_full):
        return content_matrix_full.astype(jnp.float32).reshape(
            length, subspace_batches, subspace_dimension
        )

    def to_blocks(content_matrix_full):
        return jnp.transpose(
            content_matrix_full.reshape(2, blocks, span, subspace_batches, subspace_dimension),
            (0, 3, 1, 2, 4),
        )

    gate_by_subspace = by_head(moved[0])
    address_by_subspace = by_head(moved[1])
    value_per_head = by_head(moved[2])
    amend_strength = jax.nn.sigmoid(correction_rate_logit).reshape(
        2, 1, subspace_batches, subspace_dimension
    )
    normed = address_by_subspace / jnp.sqrt(
        jnp.sum(address_by_subspace * address_by_subspace, -1, keepdims=True) + 1.0
    )
    decay_log = -math.exp(-0.5) * jax.nn.sigmoid(
        jnp.stack([by_head(moved[3]), jnp.flip(by_head(moved[4]), 0)], 0)
    )
    block_rate = jnp.transpose(amend_strength, (0, 2, 1, 3))[:, :, :, None, :]
    probe_matrix_full = to_blocks(both_ways(gate_by_subspace))
    content_matrix_full = to_blocks(both_ways(value_per_head))
    erasers = -to_blocks(both_ways(normed))
    writers = -erasers * block_rate
    rated_keys = to_blocks(both_ways(address_by_subspace)) * block_rate
    log_decay = to_blocks(decay_log)
    inclusive = jnp.cumsum(log_decay, axis=3)
    previous = inclusive - log_decay
    middle = inclusive[:, :, :, span // 2 : span // 2 + 1]
    final = inclusive[:, :, :, span - 1 : span]
    erase_query = erasers * jnp.exp(previous - middle)
    read_query = probe_matrix_full * jnp.exp(inclusive - middle)
    write_key = writers * jnp.exp(middle - inclusive)
    plain_key = rated_keys * jnp.exp(middle - inclusive)
    strict = jnp.tril(jnp.ones((span, span), jnp.bool_), -1)
    lower = jnp.tril(jnp.ones((span, span), jnp.bool_))
    erase_write = jnp.where(strict, contract("...tn,...jn->...tj", erase_query, write_key), 0.0)
    erase_plain = jnp.where(strict, contract("...tn,...jn->...tj", erase_query, plain_key), 0.0)
    read_write = jnp.where(lower, contract("...tn,...jn->...tj", read_query, write_key), 0.0)
    read_plain = jnp.where(lower, contract("...tn,...jn->...tj", read_query, plain_key), 0.0)
    identity = jnp.eye(span, dtype=jnp.float32)
    inverse = lax.linalg.triangular_solve(
        identity - erase_write,
        jnp.broadcast_to(identity, erase_write.shape),
        left_side=True,
        lower=True,
        unit_diagonal=True,
    )
    to_end = jnp.exp(final - inclusive)
    carried = contract("...jt,...jn->...tn", inverse, writers * to_end)
    start_erase = erasers * jnp.exp(previous)
    transfer = contract("...tm,...tn->...mn", start_erase, carried) + jnp.eye(
        subspace_dimension, dtype=jnp.float32
    ) * jnp.exp(final)
    inject = contract(
        "...tv,...tn->...vn",
        content_matrix_full,
        contract("...jt,...jn->...tn", erase_plain, carried) + rated_keys * to_end,
    )
    start_state = jnp.zeros(
        (2, subspace_batches, subspace_dimension, subspace_dimension), jnp.float32
    )
    _, entering = lax.scan(
        advance, start_state, (jnp.moveaxis(transfer, 2, 0), jnp.moveaxis(inject, 2, 0))
    )
    entering = jnp.moveaxis(entering, 0, 2)
    pulled = contract(
        "...tj,...jv->...tv",
        inverse,
        contract("...tk,...vk->...tv", start_erase, entering)
        + contract("...tj,...jv->...tv", erase_plain, content_matrix_full),
    )
    outputs = (
        contract("...tk,...vk->...tv", probe_matrix_full * jnp.exp(inclusive), entering)
        + contract("...tj,...jv->...tv", read_write, pulled)
        + contract("...tj,...jv->...tv", read_plain, content_matrix_full)
    )
    ordered = jnp.transpose(outputs, (0, 2, 3, 1, 4)).reshape(
        2, length, subspace_batches, subspace_dimension
    )
    ordered = jnp.stack([ordered[0], jnp.flip(ordered[1], 0)], 0)
    centred = ordered - jnp.mean(ordered, -1, keepdims=True)
    variance = jnp.mean(centred * centred, -1, keepdims=True)
    gain = head_norm_gain.reshape(1, 1, subspace_batches, subspace_dimension)
    normalized = centred * lax.rsqrt(variance + 0.00064) * gain
    diagonal_extra = diagonal_address_factor.reshape(2, 1, subspace_batches, subspace_dimension)
    diagonal_contribution = (
        jnp.sum(
            gate_by_subspace * address_by_subspace * amend_strength * diagonal_extra,
            -1,
            keepdims=True,
        )
        * value_per_head
    )
    mixed = (
        jnp.sum(normalized + diagonal_contribution, 0)
        .reshape(length, local_channels)
        .astype(jnp.bfloat16)
    )
    returned = lax.all_to_all(mixed, "sp", split_axis=0, concat_axis=1, tiled=True)
    return returned.reshape(1, row_count, channels)


def solution(mesh):
    in_specs = (
        P("dp", "sp", None),
        P("dp", None),
        P("dp", None),
        P("dp", None),
        P("dp", None),
        P(),
        P(),
        P(None, "sp"),
        P(None, "sp"),
        P("sp"),
    )
    out_specs = P("dp", "sp", None)
    return jax.shard_map(
        per_device, mesh=mesh, in_specs=in_specs, out_specs=out_specs, check_vma=False
    )
```

profile of v0, /device:TPU:4, one launch (start us, length us, event | category | flops | bytes accessed | tf_op | source)
XLA Modules:
  0.0 680.4 jit_solution(5575840417447938390)
XLA Ops:
  9.3 86.2 %all-gather.2.cloned.1.call-done = bf16[2048,3328]{1,0:T(8,128)(2,1)} async-done(((bf16[64,3328]{1,0:T(8,128)(2,1)}), bf16[2048,3328]{1,0:T(8,128)(2,1)}) %all-gather.2.cloned.1.call-update) | async-done | bytes 13631504 | tf_op jit(solution)/shard_map/all_gather | solution.py:13
  98.3 12.3 %all-to-all-start.1 = ((bf16[128,16,64]{0,2,1:T(8,128)(2,1)}), bf16[128,16,64]{0,2,1:T(8,128)(2,1)S(1)}, u32[]{:S(2)}, u32[]{:S(2)}) async-start(bf16[128,16,64]{0,2,1:T(8,128)(2,1)} %bitcast.15), calls=%async_computation.1 | async-start | bytes 524288 | tf_op jit(solution)/shard_map/all_to_all | solution.py:87
  110.6 4.2 fusion.63
  114.8 14.4 %all-to-all-done.1 = bf16[128,16,64]{0,2,1:T(8,128)(2,1)S(1)} async-done(((bf16[128,16,64]{0,2,1:T(8,128)(2,1)}), bf16[128,16,64]{0,2,1:T(8,128)(2,1)S(1)}, u32[]{:S(2)}, u32[]{:S(2)}) %all-to-all-start.1) | async-done | bytes 262176 | tf_op jit(solution)/shard_map/all_to_all | solution.py:87
  129.2 6.0 all-to-all-start.4
  135.2 4.3 fusion.60
  139.4 14.1 %all-to-all-done.4 = bf16[128,16,64]{0,2,1:T(8,128)(2,1)S(1)} async-done(((bf16[128,16,64]{0,2,1:T(8,128)(2,1)}), bf16[128,16,64]{0,2,1:T(8,128)(2,1)S(1)}, u32[]{:S(2)}, u32[]{:S(2)}) %all-to-all-start.4) | async-done | bytes 262176 | tf_op jit(solution)/shard_map/all_to_all | solution.py:86
  153.5 5.9 all-to-all-start.3
  159.5 4.2 fusion.57
  163.7 14.3 %all-to-all-done.3 = bf16[128,16,64]{0,2,1:T(8,128)(2,1)S(1)} async-done(((bf16[128,16,64]{0,2,1:T(8,128)(2,1)}), bf16[128,16,64]{0,2,1:T(8,128)(2,1)S(1)}, u32[]{:S(2)}, u32[]{:S(2)}) %all-to-all-start.3) | async-done | bytes 262176 | tf_op jit(solution)/shard_map/all_to_all | solution.py:85
  178.0 5.6 all-to-all-start
  184.8 17.2 %all-to-all-done = bf16[128,16,64]{0,2,1:T(8,128)(2,1)S(1)} async-done(((bf16[128,16,64]{0,2,1:T(8,128)(2,1)}), bf16[128,16,64]{0,2,1:T(8,128)(2,1)S(1)}, u32[]{:S(2)}, u32[]{:S(2)}) %all-to-all-start) | async-done | bytes 262176 | tf_op jit(solution)/shard_map/all_to_all | solution.py:84
  202.1 5.6 all-to-all-start.2
  212.8 5.7 reverse.14
  220.9 5.3 all-to-all-done.2
  227.0 6.7 reverse.13
  239.3 6.7 reverse.12
  254.9 3.2 copy.187
  262.0 7.6 %fusion.87 = f32[2,32,64,64]{3,2,1,0:T(8,128)} fusion(f32[1,32,64,64]{3,2,1,0:T(8,128)S(1)} %bitcast.228, f32[1,32,64,64]{3,2,1,0:T(8,128)S(1)} %bitcast.225, f32[2,1,32,64,64]{4,2,3,1,0:T(8,128)S(1)} %fusion.117, f32[2,32,64]{2,1,0:T(8,128)S(1)} %get-tuple-element.72, f32[1,32,64,64]{3,2,1,0:T(8,128)S(1)} %bitcast.241, ...), kind=kOutput, calls=%fused_computation.119 | convolution fusion | flops 203161600 | bytes 4211200 | tf_op jit(solution)/shard_map/...tn,...jn->...tj/dot_general | solution.py:21
  269.6 7.8 %fusion.89 = f32[2,32,64,64]{3,2,1,0:T(8,128)} fusion(f32[1,32,64,64]{3,2,1,0:T(8,128)S(1)} %bitcast.229, f32[1,32,64,64]{3,2,1,0:T(8,128)S(1)} %bitcast.226, f32[2,1,32,64,64]{4,2,3,1,0:T(8,128)S(1)} %fusion.117, f32[2,32,64]{2,1,0:T(8,128)S(1)} %get-tuple-element.72, f32[2,64]{1,0:T(2,128)S(1)} %add_divide_fusion, f32[1,32,64,64]{3,2,1,0:T(8,128)S(1)} %bitcast.236, ...), kind=kOutput, calls=%fused_computation.120 | convolution fusion | flops 203161600 | bytes 4211200 | tf_op jit(solution)/shard_map/...tn,...jn->...tj/dot_general | solution.py:21
  277.4 8.0 %fusion.85 = f32[2,32,64,64]{3,2,1,0:T(8,128)} fusion(f32[2,32,64]{2,1,0:T(8,128)S(1)} %get-tuple-element.72, f32[1,32,64,64]{3,2,1,0:T(8,128)S(1)} %bitcast.237, f32[1,32,64,64]{3,2,1,0:T(8,128)S(1)} %broadcast_divide_fusion, f32[1,32,64,64]{3,2,1,0:T(8,128)S(1)} %bitcast.242, f32[1,32,64,64]{3,2,1,0:T(8,128)S(1)} %bitcast.233, ...), kind=kOutput, calls=%fused_computation.117 | convolution fusion | flops 204996608 | bytes 5259776 | tf_op jit(solution)/shard_map/...tn,...jn->...tj/dot_general | solution.py:21
  285.4 8.3 %fusion.86 = f32[2,32,64,64]{3,2,1,0:T(8,128)} fusion(f32[2,32,64]{2,1,0:T(8,128)S(1)} %get-tuple-element.72, f32[1,32,64,64]{3,2,1,0:T(8,128)S(1)} %bitcast.238, f32[1,32,64,64]{3,2,1,0:T(8,128)S(1)} %broadcast_divide_fusion, f32[2,1,32,64,64]{4,2,3,1,0:T(8,128)S(1)} %fusion.117, f32[2,64]{1,0:T(2,128)S(1)} %add_divide_fusion, ...), kind=kOutput, calls=%fused_computation.118 | convolution fusion | flops 204996608 | bytes 4211200 | tf_op jit(solution)/shard_map/...tn,...jn->...tj/dot_general | solution.py:21
  304.2 3.8 copy.210
  308.1 3.9 copy.215
  311.9 3.9 copy.196
  315.8 7.9 %broadcast_select_fusion.1 = (f32[2,32,64,64]{1,3,2,0:T(8,128)}, f32[2,1,32,1,64,64]{2,5,4,3,1,0:T(8,128)}) fusion(f32[2,32,64,64]{1,3,2,0:T(8,128)} %copy.210, pred[64,64]{1,0:T(8,128)(4,1)S(1)} %get-tuple-element.87, f32[64,64]{1,0:T(8,128)S(1)} %fusion.96, f32[2,32,64,64]{1,3,2,0:T(8,128)} %copy.196, f32[64,64]{1,0:T(8,128)S(1)} %get-tuple-element.88), kind=kLoop, calls=%fused_computation.54 | loop fusion | flops 1310720 | bytes 4231168 | tf_op jit(solution)/shard_map/jit(_where)/select_n | solution.py:138
  323.7 4.1 copy.217
  327.8 3.8 copy.220
  331.6 6.4 broadcast_select_fusion
  338.0 4.1 copy.219
  342.2 4.1 copy.221
  346.3 134.0 %custom-call.3 = f32[2,1,32,1,64,64]{2,4,5,3,1,0:T(8,128)} custom-call(f32[2,1,32,1,64,64]{2,5,4,3,1,0:T(8,128)} %get-tuple-element.80), custom_call_target="InvertDiagBlocksLowerTriangular" | custom-call | tf_op jit(solution)/shard_map/triangular_solve | solution.py:142
  480.3 5.4 copy.197
  485.7 3.7 fusion.69
  490.8 4.9 fusion.33
  495.7 6.5 fusion.80
  502.2 4.0 fusion.118
  506.3 4.8 fusion.51
  511.1 4.8 fusion.50
  515.9 5.2 fusion.42
  521.1 3.9 copy.202
  525.0 4.0 add_bitcast_fusion
  529.0 5.3 copy.212
  534.3 84.6 %while.12 = (s32[]{:T(128)}, f32[2,1,64,64]{2,3,0,1:T(8,128)S(1)}, f32[32,2,1,64,64]{3,4,1,2,0:T(8,128)}, f32[32,2,1,64,64]{3,4,1,2,0:T(8,128)}, f32[32,2,1,64,64]{4,3,0,1,2:T(8,128)}, /*index=5*/s32[]{:T(128)}) while((s32[]{:T(128)}, f32[2,1,64,64]{2,3,0,1:T(8,128)S(1)}, f32[32,2,1,64,64]{3,4,1,2,0:T(8,128)}, ...), condition=%wide.region_3.4_spmd, body=%wide.region_2.3_spmd.sunk | while | flops 6299650 | bytes 458841 | solution.py:163
  618.9 6.8 %fusion.35 = f32[2,32,64,64]{3,2,1,0:T(8,128)S(1)} fusion(f32[1,32,64,64]{3,2,1,0:T(8,128)} %bitcast.235, f32[1,32,64,64]{3,2,1,0:T(8,128)} %copy-done.15, f32[1,32,64,64]{3,2,1,0:T(8,128)} %bitcast.254, f32[1,32,64,64]{3,2,1,0:T(8,128)} %bitcast.250, f32[2,1,32,64,64]{4,2,3,1,0:T(8,128)S(1)} %fusion.117, f32[32,2,1,64,64]{3,4,1,2,0:T(8,128)} %get-tuple-element.32), kind=kOutput, calls=%fused_computation.58 | convolution fusion | flops 203685888 | bytes 5242880 | tf_op jit(solution)/shard_map/...tk,...vk->...tv/dot_general | solution.py:21
  631.0 4.2 add_add_fusion
  636.3 6.8 %rev.12 = f32[2048,1,64]{2,0,1:T(8,128)S(1)} reverse(f32[2048,1,64]{2,0,1:T(8,128)} %bitcast.247), dimensions={0} | reverse | bytes 1048576 | tf_op jit(solution)/shard_map/jit(_flip)/rev | solution.py:181
  647.8 24.7 %all_to_all.78 = bf16[16,128,64]{1,2,0:T(8,128)(2,1)S(1)} all-to-all(bf16[16,128,64]{1,2,0:T(8,128)(2,1)S(1)} %copy_bitcast_fusion.4), channel_id=1, replica_groups=mesh['sp'=16,'dp'=32] {'sp'}, dimensions={0} | all-to-all | bytes 524288 | tf_op jit(solution)/shard_map/all_to_all | solution.py:200
  (298 shorter events, 140.3 us)
Async XLA Ops:
  6.5 89.0 %copy-start = (bf16[1,128,2048]{2,1,0:T(8,128)(2,1)S(1)}, bf16[1,128,2048]{2,1,0:T(8,128)(2,1)}, u32[]{:S(2)}) copy-start(bf16[1,128,2048]{2,1,0:T(8,128)(2,1)} %param.12) | copy-start | bytes 1572868
  6.5 90.7 %copy-start.32 = (bf16[2,128,1024]{2,1,0:T(8,128)(2,1)S(1)}, bf16[2,128,1024]{2,1,0:T(8,128)(2,1)}, u32[]{:S(2)}) copy-start(bf16[2,128,1024]{2,1,0:T(8,128)(2,1)} %param.17) | copy-start | bytes 1572868
  6.5 89.0 %all-gather.2.cloned.1.call-start = ((), (), s32[]{:S(2)}) async-start(), calls=%async_computation.6 | async-start | bytes 14057472 | tf_op jit(solution)/shard_map/all_gather | solution.py:13
  98.3 30.9 %all-to-all-start.1 = ((bf16[128,16,64]{0,2,1:T(8,128)(2,1)}), bf16[128,16,64]{0,2,1:T(8,128)(2,1)S(1)}, u32[]{:S(2)}, u32[]{:S(2)}) async-start(bf16[128,16,64]{0,2,1:T(8,128)(2,1)} %bitcast.15), calls=%async_computation.1 | async-start | bytes 524288 | tf_op jit(solution)/shard_map/all_to_all | solution.py:87
  129.2 24.3 %all-to-all-start.4 = ((bf16[128,16,64]{0,2,1:T(8,128)(2,1)}), bf16[128,16,64]{0,2,1:T(8,128)(2,1)S(1)}, u32[]{:S(2)}, u32[]{:S(2)}) async-start(bf16[128,16,64]{0,2,1:T(8,128)(2,1)} %bitcast.38), calls=%async_computation.4 | async-start | bytes 524288 | tf_op jit(solution)/shard_map/all_to_all | solution.py:86
  153.5 24.5 %all-to-all-start.3 = ((bf16[128,16,64]{0,2,1:T(8,128)(2,1)}), bf16[128,16,64]{0,2,1:T(8,128)(2,1)S(1)}, u32[]{:S(2)}, u32[]{:S(2)}) async-start(bf16[128,16,64]{0,2,1:T(8,128)(2,1)} %bitcast.23), calls=%async_computation.3 | async-start | bytes 524288 | tf_op jit(solution)/shard_map/all_to_all | solution.py:85
  159.5 24.1 %copy-start.34 = (f32[2,64]{1,0:T(2,128)S(1)}, f32[2,64]{1,0:T(2,128)}, u32[]{:S(2)}) copy-start(f32[2,64]{1,0:T(2,128)} %param.19) | copy-start | bytes 1540
  178.0 24.1 %all-to-all-start = ((bf16[128,16,64]{0,2,1:T(8,128)(2,1)}), bf16[128,16,64]{0,2,1:T(8,128)(2,1)S(1)}, u32[]{:S(2)}, u32[]{:S(2)}) async-start(bf16[128,16,64]{0,2,1:T(8,128)(2,1)} %bitcast.8), calls=%async_computation | async-start | bytes 524288 | tf_op jit(solution)/shard_map/all_to_all | solution.py:84
  202.1 24.1 %all-to-all-start.2 = ((bf16[128,16,64]{0,2,1:T(8,128)(2,1)}), bf16[128,16,64]{0,2,1:T(8,128)(2,1)S(1)}, u32[]{:S(2)}, u32[]{:S(2)}) async-start(bf16[128,16,64]{0,2,1:T(8,128)(2,1)} %bitcast.19), calls=%async_computation.2 | async-start | bytes 524288 | tf_op jit(solution)/shard_map/all_to_all | solution.py:88
  246.0 3.9 copy-start.26
  258.1 2.0 copy-start.11
  258.1 2.3 copy-start.17
  260.0 1.3 copy-start.5
  260.0 2.0 copy-start.7
  260.4 25.0 %copy-start.15 = (f32[1,32,64,64]{3,2,1,0:T(8,128)}, f32[1,32,64,64]{3,2,1,0:T(8,128)S(1)}, u32[]{:S(2)}) copy-start(f32[1,32,64,64]{3,2,1,0:T(8,128)S(1)} %broadcast_divide_fusion) | copy-start | bytes 1572868
  262.0 7.6 %copy-start.13 = (f32[2048,1,64]{2,0,1:T(8,128)S(1)}, f32[2048,1,64]{2,0,1:T(8,128)}, u32[]{:S(2)}) copy-start(f32[2048,1,64]{2,0,1:T(8,128)} %copy.236) | copy-start | bytes 1572868
  269.6 7.8 %copy-start.28 = (f32[16,128,64]{2,1,0:T(8,128)S(1)}, f32[16,128,64]{2,1,0:T(8,128)}, u32[]{:S(2)}) copy-start(f32[16,128,64]{2,1,0:T(8,128)} %copy.237) | copy-start | bytes 1572868
  269.6 7.8 %copy-start.30 = (f32[2048,64]{1,0:T(8,128)S(1)}, f32[2048,64]{1,0:T(8,128)}, u32[]{:S(2)}) copy-start(f32[2048,64]{1,0:T(8,128)} %copy.238) | copy-start | bytes 1572868
  285.4 8.3 %copy-start.25 = (f32[16,128,64]{1,2,0:T(8,128)S(1)}, f32[16,128,64]{1,2,0:T(8,128)}, u32[]{:S(2)}) copy-start(f32[16,128,64]{1,2,0:T(8,128)} %get-tuple-element.73) | copy-start | bytes 1572868
  294.8 5.1 copy-start.24
  485.7 5.0 copy-start.14
  485.7 5.0 copy-start.16
  489.4 1.3 copy-start.3
  490.8 4.9 copy-start.29
  490.8 4.9 copy-start.31
  495.7 6.5 copy-start.2
  502.2 4.0 copy-start.9
  502.2 4.0 copy-start.10
  506.2 4.8 copy-start.20
  511.1 4.8 copy-start.12
  511.1 4.8 copy-start.18
  618.9 6.8 %copy-start.4 = (f32[2,32,64,64]{3,2,1,0:T(8,128)S(1)}, f32[2,32,64,64]{3,2,1,0:T(8,128)}, u32[]{:S(2)}) copy-start(f32[2,32,64,64]{3,2,1,0:T(8,128)} %copy-done.3) | copy-start | bytes 3145732
  618.9 6.8 %copy-start.22 = (f32[2,32,64,64]{3,2,1,0:T(8,128)S(1)}, f32[2,32,64,64]{3,2,1,0:T(8,128)}, u32[]{:S(2)}) copy-start(f32[2,32,64,64]{3,2,1,0:T(8,128)} %fusion.51) | copy-start | bytes 3145732
  625.8 2.3 copy-start.19
  628.1 2.4 copy-start.6
  628.1 2.4 copy-start.8
  628.1 2.4 copy-start.21
  628.1 2.8 copy-start.27
  643.2 2.0 copy-start.33
  643.2 2.2 copy-start.23
  643.2 2.2 copy-start.35
  645.4 27.9 %copy-start.1 = (bf16[1,128,2048]{2,1,0:T(8,128)(2,1)S(1)}, bf16[1,128,2048]{2,1,0:T(8,128)(2,1)}, u32[]{:S(2)}) copy-start(bf16[1,128,2048]{2,1,0:T(8,128)(2,1)} %param.12) | copy-start | bytes 1572868
Sparse Core Ops, SparseCore 0:
  10.5 84.9 all-gather.1
where the time goes:
time: 694 us; the launch traced here: 680 us
  other arithmetic  165 us (24%)
  local copies, waits for them, and re-layouts  159 us (23%)
  waiting for transfers between devices  152 us (22%)
  matrix products  129 us (19%)
  starting transfers between devices  35.3 us (5%)
  blocking collectives  24.7 us (4%)
  between operations  14.3 us (2%)
    another operation x4, other arithmetic, per_device(): lax.linalg.triangular_solve(identity - erase_write, jnp.broadcast_to(iden...  134 us
    dot_general x46, matrix products, contract(): return jnp.einsum(pattern, former, latter, precision=lax.Precision.HIGHEST)  110 us
    all_gather x1, waiting for transfers between devices, in_one_piece(): result, at, outs = (lax.all_gather(both, axis, axis=dim, tiled=True), 0, [])  86.2 us
    dynamic_slice x64, local copies, waits for them, and re-layouts, per_device(): lax.scan(advance, start_state, (jnp.moveaxis(transfer, 2, 0), jnp.moveaxi...  29.9 us
    another operation x5, local copies, waits for them, and re-layouts  25.8 us
    all_to_all x1, blocking collectives, per_device(): lax.all_to_all(mixed, 'sp', split_axis=0, concat_axis=1, tiled=True)  24.7 us
    dynamic_update_slice x32, local copies, waits for them, and re-layouts, per_device(): lax.scan(advance, start_state, (jnp.moveaxis(transfer, 2, 0), jnp.moveaxi...  20.4 us
    dot_general x5, local copies, waits for them, and re-layouts, contract(): return jnp.einsum(pattern, former, latter, precision=lax.Precision.HIGHEST)  19.3 us
  transfers between devices with their start and end apart: 6, of which 6 were waited for; matrix products, arithmetic and copies ran while one was open for 4% of the time, Pallas kernels for 0%

commit v1 on v0

v1 whole, which is shorter than its diff:
```python
import math
import functools
import jax
import jax.numpy as jnp
from jax import lax
from jax.experimental import pallas as pl
from jax.experimental.pallas import tpu as pltpu
from jax.sharding import PartitionSpec as P

BF = jnp.bfloat16
F32 = jnp.float32
C = 128
H = 64


def split2(x):
    hi = x.astype(BF)
    return hi, (x - hi.astype(F32)).astype(BF)


def left3(a):
    hi, lo = split2(a)
    return jnp.concatenate([hi, lo], 1)


def right3(b):
    hi, lo = split2(b)
    return jnp.concatenate(
        [jnp.concatenate([hi, lo], 1), jnp.concatenate([hi, jnp.zeros_like(lo)], 1)], 0
    )


def dot3(a3, b3):
    t = jnp.dot(a3, b3, preferred_element_type=F32)
    n = t.shape[1] // 2
    return t[:, :n] + t[:, n:]


def nt(a, b):
    return lax.dot_general(a, b, (((1,), (1,)), ((), ())), preferred_element_type=F32)


def tn(a, b):
    return lax.dot_general(a, b, (((0,), (0,)), ((), ())), preferred_element_type=F32)


def head_ones(scale=1.0):
    r = lax.broadcasted_iota(jnp.int32, (256, 128), 0)
    c = lax.broadcasted_iota(jnp.int32, (256, 128), 1)
    return jnp.where(((r >> 6) & 1) == (c >> 6), scale, 0.0).astype(BF)


def head_sum(x, ones):
    hi, lo = split2(x)
    return jnp.dot(jnp.concatenate([hi, lo], 1), ones, preferred_element_type=F32)


def product(a, b):
    return dot3(left3(a), right3(b))


def prep_kernel(q_ref, k_ref, v_ref, low_ref, up_ref, floor_ref, rate_ref, msg_ref, y_ref, qx_ref):
    chunks = q_ref.shape[0] // C
    q = q_ref[...].astype(F32)
    k = k_ref[...].astype(F32)
    v = v_ref[...].astype(F32)
    row = lax.broadcasted_iota(jnp.int32, (C, C), 0)
    col = lax.broadcasted_iota(jnp.int32, (C, C), 1)
    x = row ^ col
    left = lax.broadcasted_iota(jnp.int32, (C, C), 1) < H
    ones = head_ones()
    inv = 1.0 / (1.0 + head_sum(k * k, ones))
    nk = -(k * inv)
    probs = []
    for d in range(2):
        pre = (
            jnp.dot(low_ref[:, d * 128 : (d + 1) * 128], up_ref[d], preferred_element_type=F32)
            + floor_ref[d : d + 1, :]
        ).astype(BF).astype(F32)
        logd = -math.exp(-0.5) * jax.nn.sigmoid(pre)
        rate = jax.nn.sigmoid(rate_ref[d : d + 1, :])
        kap = k * rate
        strict = (col < row) if d == 0 else (col > row)
        tri = jnp.where((col <= row) if d == 0 else (col >= row), 1.0, 0.0).astype(BF)
        for ci in range(chunks):
            c = ci if d == 0 else chunks - 1 - ci
            sl = slice(c * C, (c + 1) * C)
            ld = logd[sl]
            hi, lo = split2(ld)
            cs = jnp.dot(tri, jnp.concatenate([hi, lo], 1), preferred_element_type=F32)
            inc = cs[:, :128] + cs[:, 128:]
            mid = inc[C // 2 : C // 2 + 1]
            fin = inc[C - 1 : C] if d == 0 else inc[0:1]
            rel = inc - mid
            up_e = jnp.exp(rel)
            gq = nk[sl] * jnp.exp(rel - ld)
            rq = q[sl] * up_e
            pk = kap[sl] * jnp.exp(-rel)
            emid = jnp.exp(mid)
            ke = pk * jnp.exp(fin - mid)
            g0 = gq * emid
            r0 = rq * emid
            gl = pltpu.roll(g0, H, 1)
            vs = v[sl]
            pkh, pkl = split2(pk)
            rhs = jnp.concatenate(
                [jnp.concatenate([pkh, pkh], 1), jnp.concatenate([pkl, jnp.zeros_like(pkl)], 1)], 0
            )
            zero = jnp.zeros_like(gq)
            att = nt(
                jnp.concatenate(
                    [
                        left3(jnp.where(left, gq, zero)),
                        left3(jnp.where(left, rq, zero)),
                        left3(jnp.where(left, zero, gq)),
                        left3(jnp.where(left, zero, rq)),
                    ],
                    0,
                ),
                rhs,
            )
            att = att[:, :C] + att[:, C:]
            heads = []
            for a in range(2):
                m = jnp.where(strict, att[2 * a * C : (2 * a + 1) * C], 0.0)
                r = jnp.where(tri > 0, att[(2 * a + 1) * C : (2 * a + 2) * C], 0.0)
                b = jnp.where(left, vs, gl) if a == 0 else jnp.where(left, gl, vs)
                heads.append(dict(m=m, r=r, b=b))
            probs.append(
                dict(d=d, c=c, heads=heads, ke=ke, r0=r0, fin=fin)
            )
    allh = [h for p in probs for h in p["heads"]]
    for h in allh:
        h["n"] = jnp.where(x == 1, h["m"], 0.0)
    for lb in range(1, 7):
        sel = (x >> lb) == 1
        for h in allh:
            h["off"] = jnp.where(sel, h["m"], 0.0)
            h["w"] = h["off"] + product(h["off"], h["n"])
        for h in allh:
            h["n"] = h["n"] + h["w"] + product(h["n"], h["w"])
    for h in allh:
        h["x"] = h["b"] + dot3(left3(h["n"]), right3(h["b"]))
    row2 = lax.broadcasted_iota(jnp.int32, (C, C), 0)
    for d in range(2):
        u = None
        for ci in range(chunks):
            p = probs[d * chunks + ci]
            sl = slice(p["c"] * C, (p["c"] + 1) * C)
            xa, xb = p["heads"][0]["x"], p["heads"][1]["x"]
            ya = dot3(left3(p["heads"][0]["r"]), right3(xa))
            yb = dot3(left3(p["heads"][1]["r"]), right3(xb))
            y0 = jnp.where(left, ya, yb)
            qx = p["r0"] + pltpu.roll(jnp.where(left, yb, ya), H, 1)
            kh, kl = split2(
                jnp.concatenate([jnp.where(left, p["ke"], 0.0), jnp.where(left, 0.0, p["ke"])], 0)
            )
            xh, xl = split2(jnp.concatenate([xa, xb], 0))
            un = tn(kh, jnp.concatenate([xh, xl], 1))
            un = un[:, :C] + un[:, C:] + tn(kl, xh)
            un = jnp.where(row2 < H, un, pltpu.roll(un, H, 1))
            ef = jnp.exp(p["fin"])
            efr = pltpu.roll(jnp.broadcast_to(ef, (C, C)), H, 1)
            dm = jnp.where(row2 < H, efr, jnp.broadcast_to(ef, (C, C)))
            un = un + jnp.where(col == (row2 & (H - 1)) + H, dm, 0.0)
            if u is None:
                u = un
            else:
                uh, ul = split2(u)
                ub_i = jnp.where(row2 < H, jnp.where(left, u, 0.0), jnp.where(left, 0.0, pltpu.roll(u, H, 1)))
                ub_t = jnp.where(row2 < H, jnp.where(left, pltpu.roll(u, H, 1), 0.0), jnp.where(left, 0.0, u))
                bh, bl = split2(jnp.concatenate([ub_i, ub_t], 1))
                q3 = left3(qx)
                qd = jnp.dot(
                    q3, jnp.concatenate([bh, bh], 0), preferred_element_type=F32
                ) + jnp.dot(q3[:, :C], bl, preferred_element_type=F32)
                y0 = y0 + qd[:, :C]
                qx = qd[:, C:]
                tl = jnp.where(left, 0.0, un)
                t2 = jnp.where(row2 < H, jnp.where(left, pltpu.roll(un, H, 1), 0.0), tl)
                th, tlo = split2(t2)
                lhs = jnp.concatenate([th, tlo], 1)
                comp = (
                    jnp.dot(lhs, jnp.concatenate([uh, uh], 0), preferred_element_type=F32)
                    + jnp.dot(th, ul, preferred_element_type=F32)
                )
                u = comp + jnp.where(left, un, 0.0)
            y_ref[d, sl, :] = y0
            qx_ref[d, sl, :] = qx
        msg_ref[d] = u[:H].astype(BF)
        msg_ref[2 + d] = u[H:].astype(BF)


def prep(qkv, low, up, floor, rate, tokens):
    rows, width3 = qkv.shape
    width = width3 // 3
    seqs = rows // tokens
    hps = width // 128
    grid = (seqs, hps)
    sb = lambda off: pl.BlockSpec((tokens, 128), lambda s, h: (s, h + off * hps))
    return pl.pallas_call(
        prep_kernel,
        grid=grid,
        in_specs=[
            sb(0),
            sb(1),
            sb(2),
            pl.BlockSpec((tokens, 256), lambda s, h: (s, 0)),
            pl.BlockSpec((2, 128, 128), lambda s, h: (0, 0, h)),
            pl.BlockSpec((2, 128), lambda s, h: (0, h)),
            pl.BlockSpec((2, 128), lambda s, h: (0, h)),
        ],
        out_specs=[
            pl.BlockSpec((4, H, 128), lambda s, h: (s * hps + h, 0, 0)),
            pl.BlockSpec((2, tokens, 128), lambda s, h: (0, s, h)),
            pl.BlockSpec((2, tokens, 128), lambda s, h: (0, s, h)),
        ],
        out_shape=[
            jax.ShapeDtypeStruct((seqs * hps * 4, H, 128), BF),
            jax.ShapeDtypeStruct((2, rows, width), F32),
            jax.ShapeDtypeStruct((2, rows, width), F32),
        ],
        compiler_params=pltpu.CompilerParams(vmem_limit_bytes=56 * 1024 * 1024),
        name="prep",
    )(qkv, qkv, qkv, low, up, floor, rate)


def final_kernel(y_ref, qx_ref, s_ref, q_ref, k_ref, v_ref, rate_ref, diag_ref, gain_ref, o_ref):
    q = q_ref[...].astype(F32)
    k = k_ref[...].astype(F32)
    v = v_ref[...].astype(F32)
    mean = head_ones(1.0 / H)
    ones = head_ones()
    wt = jax.nn.sigmoid(rate_ref[0:1]) * diag_ref[0:1] + jax.nn.sigmoid(rate_ref[1:2]) * diag_ref[1:2]
    own = head_sum(q * k * wt, ones) * v
    total = own
    z = jnp.zeros((H, H), BF)
    for d in range(2):
        sa, sb = s_ref[d], s_ref[2 + d]
        blk = jnp.concatenate(
            [
                jnp.concatenate([jnp.concatenate([sa[:, :H], sa[:, H:]], 0), z], 1),
                jnp.concatenate([z, jnp.concatenate([sb[:, :H], sb[:, H:]], 0)], 1),
            ],
            0,
        )
        y = y_ref[d] + jnp.dot(
            left3(qx_ref[d]), jnp.concatenate([blk, blk], 0), preferred_element_type=F32
        )
        cen = y - head_sum(y, mean)
        var = head_sum(cen * cen, mean)
        total = total + cen * lax.rsqrt(var + 0.00064) * gain_ref[...]
    o_ref[...] = total.astype(BF)


def final(y, qx, s, qkv, rate, diag, gain, tokens):
    rows, width3 = qkv.shape
    width = width3 // 3
    seqs = rows // tokens
    hps = width // 128
    sb = lambda off: pl.BlockSpec((tokens, 128), lambda s, h: (s, h + off * hps))
    dspec = pl.BlockSpec((2, tokens, 128), lambda s, h: (0, s, h))
    par = pl.BlockSpec((2, 128), lambda s, h: (0, h))
    return pl.pallas_call(
        final_kernel,
        grid=(seqs, hps),
        in_specs=[
            dspec,
            dspec,
            pl.BlockSpec((4, 32, 128), lambda s, h: (s * hps + h, 0, 0)),
            sb(0),
            sb(1),
            sb(2),
            par,
            par,
            pl.BlockSpec((1, 128), lambda s, h: (0, h)),
        ],
        out_specs=pl.BlockSpec((tokens, 128), lambda s, h: (s, h)),
        out_shape=jax.ShapeDtypeStruct((rows, width), BF),
        compiler_params=pltpu.CompilerParams(vmem_limit_bytes=56 * 1024 * 1024),
        name="final",
    )(y, qx, s, qkv, qkv, qkv, rate, diag, gain)


def scan_kernel(roles, back_ref, u_ref, o_ref):
    groups = u_ref.shape[0] // roles
    back = back_ref[0]
    states = [jnp.zeros((H, H), F32) for _ in range(roles)]
    zero = jnp.zeros((H, 128), BF)
    for i in range(groups):
        g = jnp.where(back == 1, groups - 1 - i, i)
        for p in range(roles):
            src = g * roles + p
            s = states[p]
            hi, lo = split2(s)
            o_ref[src] = jnp.concatenate([hi[:32], hi[32:]], 1)
            u = u_ref[src]
            t = jnp.dot(
                u, jnp.concatenate([zero, jnp.concatenate([hi, lo], 1)], 0), preferred_element_type=F32
            )
            states[p] = u[:, :H].astype(F32) + t[:, :H] + t[:, H:]


def scan_states(u, back, roles):
    n = u.shape[0]
    return pl.pallas_call(
        functools.partial(scan_kernel, roles),
        in_specs=[pl.BlockSpec(memory_space=pltpu.SMEM), pl.BlockSpec(memory_space=pltpu.VMEM)],
        out_specs=pl.BlockSpec(memory_space=pltpu.VMEM),
        out_shape=jax.ShapeDtypeStruct((n, 32, 128), BF),
        name="states",
    )(back, u)


def project_kernel(
    idx_ref, b0, fm, fp, ot, ob, r1, r2, r3t, r3b, t0, t1, t2, t3, qkv_ref, low_ref, w_ref
):
    rows = b0.shape[0]
    half = rows // 2
    w_ref[idx_ref[0]] = b0[...]
    w_ref[idx_ref[1]] = fm[...]
    w_ref[idx_ref[2]] = fp[...]
    w_ref[idx_ref[3], :half] = ot[...]
    w_ref[idx_ref[3], half:] = ob[...]
    for i in range(4):
        w_ref[idx_ref[4 + i]] = r1[i * rows : (i + 1) * rows]
        w_ref[idx_ref[8 + i]] = r2[i * rows : (i + 1) * rows]
    for i in range(2):
        w_ref[idx_ref[12 + i]] = r3t[i * rows : (i + 1) * rows]
        w_ref[idx_ref[14 + i]] = r3b[i * rows : (i + 1) * rows]
    width3 = qkv_ref.shape[1]
    n = t0.shape[0]
    for i, t in enumerate((t0, t1, t2, t3)):
        at = pl.ds(pl.multiple_of(idx_ref[16 + i] * n, n), n)
        w = w_ref[...].reshape(-1, w_ref.shape[2])
        out = jnp.dot(t[...], w, preferred_element_type=F32)
        qkv_ref[at, :] = out[:, :width3].astype(BF)
        low_ref[at, :] = jnp.tanh(out[:, width3:]).astype(BF)


def project(idx, blocks, toks, width3):
    cols = blocks[0].shape[1]
    n = toks[0].shape[0]
    vm = pl.BlockSpec(memory_space=pltpu.VMEM)
    return pl.pallas_call(
        project_kernel,
        in_specs=[pl.BlockSpec(memory_space=pltpu.SMEM)] + [vm] * 13,
        out_specs=[vm, vm],
        out_shape=[
            jax.ShapeDtypeStruct((4 * n, width3), BF),
            jax.ShapeDtypeStruct((4 * n, cols - width3), BF),
        ],
        scratch_shapes=[pltpu.VMEM((16, blocks[0].shape[0], cols), BF)],
        compiler_params=pltpu.CompilerParams(vmem_limit_bytes=56 * 1024 * 1024),
        name="project",
    )(idx, *blocks, *toks)


def shift(first, by):
    pairs = []
    for i in range(32):
        core, j = i % 2, i // 2
        y, x = j // 4, j % 4
        if (core == 0) == first:
            x = (x + by) % 4
        else:
            y = (y + by) % 4
        pairs.append((i, (y * 4 + x) * 2 + core))
    return pairs


CORES = [(i, i ^ 1) for i in range(32)]
ZPAIRS = [(i, i ^ 1) for i in range(16)]


def body(tokens, wq, wk, wv, wd, up, floor, rate, diag, gain):
    z = lax.axis_index("sp")
    dp = lax.axis_index("dp")
    c, p = dp % 2, z % 2
    j = dp // 2
    y, x = j // 4, j % 4
    width = 256
    tok = tokens.reshape(-1, tokens.shape[2])
    n = tok.shape[0]

    def columns(role):
        cut = lambda w: lax.dynamic_slice_in_dim(w, role * width, width, 1)
        return jnp.concatenate([cut(wq), cut(wk), cut(wv), wd], 1)

    role = 2 * p + c
    keep = columns(role)
    recv = lax.ppermute(columns(2 * p + 1 - c), "dp", CORES)
    b0 = jnp.where(c == 0, jnp.concatenate([keep, recv], 0), jnp.concatenate([recv, keep], 0))
    rows = b0.shape[0]
    fm = lax.ppermute(b0, "dp", shift(True, 1))
    fp = lax.ppermute(b0, "dp", shift(True, -1))
    ot = lax.ppermute(fm[: rows // 2], "dp", shift(True, 1))
    ob = lax.ppermute(fp[rows // 2 :], "dp", shift(True, -1))
    tz = lax.ppermute(tok, "sp", ZPAIRS)
    tc = lax.ppermute(tok, "dp", CORES)
    s4 = jnp.concatenate([b0, fm, fp, ot, ob], 0)
    r1 = lax.ppermute(s4, "dp", shift(False, 1))
    r2 = lax.ppermute(s4, "dp", shift(False, -1))
    tcz = lax.ppermute(tz, "dp", CORES)
    r3t = lax.ppermute(r1[: 2 * rows], "dp", shift(False, 1))
    r3b = lax.ppermute(r2[2 * rows :], "dp", shift(False, -1))

    par = jnp.concatenate([rate, diag, gain[None], jnp.zeros((3, gain.shape[0]), F32)], 0)
    par = jnp.broadcast_to(par[None], (16,) + par.shape)
    par = lax.all_to_all(par, "sp", split_axis=0, concat_axis=0, tiled=True)
    par = lax.dynamic_slice_in_dim(par, 4 * role, 4, 0)
    par = jnp.transpose(par, (1, 0, 2)).reshape(8, width)
    rate4, diag4, gain4 = par[0:2], par[2:4], par[4:5]
    up4 = lax.dynamic_slice_in_dim(up, role * width, width, 2)
    floor4 = lax.dynamic_slice_in_dim(floor, role * width, width, 1)

    a = jnp.where(c == 0, x, y)
    b = jnp.where(c == 0, y, x)
    ids = []
    for eps in (0, -1, 1, 2):
        for delta in (0, -1, 1, 2):
            aa, bb = (a + delta) % 4, (b + eps) % 4
            ids.append(jnp.where(c == 0, bb * 4 + aa, aa * 4 + bb))
    ids += [2 * c + p, 2 * c + 1 - p, 2 * (1 - c) + p, 2 * (1 - c) + 1 - p]
    idx = jnp.stack(ids).astype(jnp.int32)
    qkv, low = project(
        idx, (b0, fm, fp, ot, ob, r1, r2, r3t, r3b), (tok, tz, tc, tcz), 3 * width
    )
    span = 2 * n
    msg, y0, qx = prep(qkv, low, up4, floor4, rate4, span)
    got = lax.all_to_all(msg, "sp", split_axis=0, concat_axis=0, tiled=True)
    st = scan_states(got, (z % 2).reshape(1).astype(jnp.int32), 2)
    st = lax.all_to_all(st, "sp", split_axis=0, concat_axis=0, tiled=True)
    out = final(y0, qx, st, qkv, rate4, diag4, gain4, span)

    out = out.reshape(2, 2, n, width)
    mine = lax.dynamic_index_in_dim(out, p, 1, False)
    rz = lax.ppermute(lax.dynamic_index_in_dim(out, 1 - p, 1, False), "sp", ZPAIRS)
    pick = lambda m, s: lax.dynamic_index_in_dim(m, s, 0, False)
    low_p = jnp.where(p == 0, mine, rz)
    high_p = jnp.where(p == 0, rz, mine)
    both = jnp.concatenate([low_p, high_p], 2)
    far = lax.ppermute(pick(both, 1 - c), "dp", CORES)
    near = pick(both, c)
    first = jnp.where(c == 0, near, far)
    second = jnp.where(c == 0, far, near)
    res = jnp.concatenate(
        [first[:, :width], second[:, :width], first[:, width:], second[:, width:]], 1
    )
    return res.reshape(1, n, 4 * width)


def solution(mesh):
    in_specs = (
        P("dp", "sp", None),
        P("dp", None),
        P("dp", None),
        P("dp", None),
        P("dp", None),
        P(),
        P(),
        P(None, "sp"),
        P(None, "sp"),
        P("sp"),
    )
    return jax.shard_map(
        body, mesh=mesh, in_specs=in_specs, out_specs=P("dp", "sp", None), check_vma=False
    )
```

time: 694 us -> 174 us (0.25)
  the two profiles are of different devices: /device:TPU:4 before, /device:TPU:1 now
where the time goes in v1:
time: 174 us; the launch traced here: 173 us
  starting transfers between devices  75.1 us (43%)
  Pallas kernels  35.4 us (20%)
  blocking collectives  25.6 us (15%)
  waiting for transfers between devices  18.7 us (11%)
  local copies, waits for them, and re-layouts  15.5 us (9%)
  other arithmetic  2.43 us (1%)
    all_to_all x1, blocking collectives, body(): got = lax.all_to_all(msg, 'sp', split_axis=0, concat_axis=0, tiled=True)  25.6 us
    pallas_call x1, Pallas kernels, prep(): pl.pallas_call(prep_kernel, grid=grid, in_specs=[sb(0), sb(1), sb(2), pl....  20.1 us
    all_to_all x1, waiting for transfers between devices, body(): st = lax.all_to_all(st, 'sp', split_axis=0, concat_axis=0, tiled=True)  10.6 us
    all_to_all x1, starting transfers between devices, body(): par = lax.all_to_all(par, 'sp', split_axis=0, concat_axis=0, tiled=True)  10.6 us
    all_to_all x1, starting transfers between devices, body(): st = lax.all_to_all(st, 'sp', split_axis=0, concat_axis=0, tiled=True)  10.3 us
    ppermute x1, starting transfers between devices, body(): recv = lax.ppermute(columns(2 * p + 1 - c), 'dp', CORES)  8.75 us
    ppermute x1, starting transfers between devices, body(): far = lax.ppermute(pick(both, 1 - c), 'dp', CORES)  6.53 us
    pallas_call x1, Pallas kernels, project(): pl.pallas_call(project_kernel, in_specs=[pl.BlockSpec(memory_space=pltpu....  6.44 us
  transfers between devices with their start and end apart: 16, of which 6 were waited for; matrix products, arithmetic and copies ran while one was open for 6% of the time, Pallas kernels for 0%

profile of v1, /device:TPU:1, one launch (start us, length us, event | category | flops | bytes accessed | tf_op | source)
XLA Modules:
  0.0 173.3 jit_solution(16468958998378961162)
XLA Ops:
  0.0 0.8 constant_dynamic-slice_fusion.4
  1.0 0.8 constant_dynamic-slice_fusion.2
  1.8 8.7 %collective-permute-start = (bf16[64,1024]{1,0:T(8,128)(2,1)S(1)}, bf16[64,1024]{1,0:T(8,128)(2,1)S(1)}, u32[]{:S(2)}, u32[]{:S(2)}) collective-permute-start(bf16[64,1024]{1,0:T(8,128)(2,1)S(1)} %pad_maximum_fusion), channel_id=1, source_target_pairs={{0,1},{1,0},{2,3},{3,2},{4,5},{5,4},{6,7},{7,6},{8,9},{9,8},{10,11... | collective-permute-start | bytes 393224 | tf_op jit(solution)/shard_map/ppermute | solution.py:392
  10.6 1.0 collective-permute-done
  11.5 0.8 constant_dynamic-update-slice_fusion.4
  12.3 1.9 %collective-permute-start.1 = (bf16[128,1024]{1,0:T(8,128)(2,1)S(1)}, bf16[128,1024]{1,0:T(8,128)(2,1)S(1)}, u32[]{:S(2)}, u32[]{:S(2)}) collective-permute-start(bf16[128,1024]{1,0:T(8,128)(2,1)S(1)} %get-tuple-element.16.b0), channel_id=1, source_target_pairs={{0,2},{1,9},{2,4},{3,11},{4,6},{5,13},{6,0},{7,15},{8,10},{9,17},{... | collective-permute-start | bytes 786440 | tf_op jit(solution)/shard_map/ppermute | solution.py:395
  14.2 4.6 %collective-permute-start.2 = (bf16[128,1024]{1,0:T(8,128)(2,1)S(1)}, bf16[128,1024]{1,0:T(8,128)(2,1)S(1)}, u32[]{:S(2)}, u32[]{:S(2)}) collective-permute-start(bf16[128,1024]{1,0:T(8,128)(2,1)S(1)} %get-tuple-element.16.b0), channel_id=1, source_target_pairs={{0,6},{1,25},{2,0},{3,27},{4,2},{5,29},{6,4},{7,31},{8,14},{9,1},{... | collective-permute-start | bytes 786440 | tf_op jit(solution)/shard_map/ppermute | solution.py:396
  18.8 2.1 %collective-permute-done.1.fm = bf16[128,1024]{1,0:T(8,128)(2,1)S(1)} collective-permute-done((bf16[128,1024]{1,0:T(8,128)(2,1)S(1)}, bf16[128,1024]{1,0:T(8,128)(2,1)S(1)}, u32[]{:S(2)}, u32[]{:S(2)}) %collective-permute-start.1) | collective-permute-done | bytes 262176 | tf_op jit(solution)/shard_map/ppermute | solution.py:395
  20.9 1.9 %collective-permute-start.3 = (bf16[64,1024]{1,0:T(8,128)(2,1)S(1)}, bf16[64,1024]{1,0:T(8,128)(2,1)S(1)}, u32[]{:S(2)}, u32[]{:S(2)}) collective-permute-start(bf16[64,1024]{1,0:T(8,128)(2,1)S(1)} %slice.56), channel_id=1, source_target_pairs={{0,2},{1,9},{2,4},{3,11},{4,6},{5,13},{6,0},{7,15},{8,10},{9,17},{... | collective-permute-start | bytes 393224 | tf_op jit(solution)/shard_map/ppermute | solution.py:397
  22.9 4.6 %collective-permute-start.4 = (bf16[64,1024]{1,0:T(8,128)(2,1)S(1)}, bf16[64,1024]{1,0:T(8,128)(2,1)S(1)}, u32[]{:S(2)}, u32[]{:S(2)}) collective-permute-start(bf16[64,1024]{1,0:T(8,128)(2,1)S(1)} %slice.57), channel_id=1, source_target_pairs={{0,6},{1,25},{2,0},{3,27},{4,2},{5,29},{6,4},{7,31},{8,14},{9,1},{... | collective-permute-start | bytes 393224 | tf_op jit(solution)/shard_map/ppermute | solution.py:398
  27.5 0.7 constant_dynamic-update-slice_fusion.3
  28.2 0.7 constant_dynamic-update-slice_fusion.2
  29.0 0.7 constant_dynamic-update-slice_fusion.1
  29.7 0.7 copy-done.9
  30.3 0.7 constant_dynamic-update-slice_fusion
  31.0 1.9 %collective-permute-start.5 = (bf16[512,1024]{1,0:T(8,128)(2,1)}, bf16[512,1024]{1,0:T(8,128)(2,1)S(1)}, u32[]{:S(2)}, u32[]{:S(2)}) collective-permute-start(bf16[512,1024]{1,0:T(8,128)(2,1)} %constant_dynamic-update-slice_fusion), channel_id=1, source_target_pairs={{0,8},{1,3},{2,10},{3,5},{4,12},{5,7},{6,14},{7,1},{8,16},{9,11},{... | collective-permute-start | bytes 3145736 | tf_op jit(solution)/shard_map/ppermute | solution.py:402
  32.9 4.6 %collective-permute-start.6 = (bf16[512,1024]{1,0:T(8,128)(2,1)}, bf16[512,1024]{1,0:T(8,128)(2,1)S(1)}, u32[]{:S(2)}, u32[]{:S(2)}) collective-permute-start(bf16[512,1024]{1,0:T(8,128)(2,1)} %constant_dynamic-update-slice_fusion), channel_id=1, source_target_pairs={{0,24},{1,7},{2,26},{3,1},{4,28},{5,3},{6,30},{7,5},{8,0},{9,15},{... | collective-permute-start | bytes 3145736 | tf_op jit(solution)/shard_map/ppermute | solution.py:403
  37.5 1.9 %collective-permute-start.9 = (bf16[128,2048]{1,0:T(8,128)(2,1)}, bf16[128,2048]{1,0:T(8,128)(2,1)S(1)}, u32[]{:S(2)}, u32[]{:S(2)}) collective-permute-start(bf16[128,2048]{1,0:T(8,128)(2,1)} %bitcast.20.t0), channel_id=1, source_target_pairs={{0,32},{32,0},{64,96},{96,64},{128,160},{160,128},{192,224},{224,1... | collective-permute-start | bytes 1572872 | tf_op jit(solution)/shard_map/ppermute | solution.py:399
  39.4 4.6 %collective-permute-start.10 = (bf16[128,2048]{1,0:T(8,128)(2,1)}, bf16[128,2048]{1,0:T(8,128)(2,1)}, u32[]{:S(2)}, u32[]{:S(2)}) collective-permute-start(bf16[128,2048]{1,0:T(8,128)(2,1)} %bitcast.20.t0), channel_id=1, source_target_pairs={{0,1},{1,0},{2,3},{3,2},{4,5},{5,4},{6,7},{7,6},{8,9},{9,8},{10,11... | collective-permute-start | bytes 1572872 | tf_op jit(solution)/shard_map/ppermute | solution.py:400
  44.1 0.7 copy-done.13
  44.8 0.7 reshape.28
  45.5 10.6 %all-to-all-start = ((f32[16,1,512]{2,1,0:T(1,128)}), f32[16,1,512]{2,1,0:T(1,128)S(1)}, u32[]{:S(2)}, u32[]{:S(2)}) async-start(f32[16,1,512]{2,1,0:T(1,128)} %reshape.28), calls=%async_computation | async-start | bytes 65536 | tf_op jit(solution)/shard_map/all_to_all | solution.py:410
  56.2 2.2 %collective-permute-start.11 = (bf16[128,2048]{1,0:T(8,128)(2,1)S(1)}, bf16[128,2048]{1,0:T(8,128)(2,1)}, u32[]{:S(2)}, u32[]{:S(2)}) collective-permute-start(bf16[128,2048]{1,0:T(8,128)(2,1)S(1)} %collective-permute-done.9.t1), channel_id=1, source_target_pairs={{0,1},{1,0},{2,3},{3,2},{4,5},{5,4},{6,7},{7,6},{8,9},{9,8},{10,11... | collective-permute-start | bytes 1572872 | tf_op jit(solution)/shard_map/ppermute | solution.py:404
  58.5 0.9 slice.58
  59.4 2.6 %collective-permute-start.7 = (bf16[256,1024]{1,0:T(8,128)(2,1)}, bf16[256,1024]{1,0:T(8,128)(2,1)}, u32[]{:S(2)}, u32[]{:S(2)}) collective-permute-start(bf16[256,1024]{1,0:T(8,128)(2,1)} %slice.58), channel_id=1, source_target_pairs={{0,8},{1,3},{2,10},{3,5},{4,12},{5,7},{6,14},{7,1},{8,16},{9,11},{... | collective-permute-start | bytes 1572872 | tf_op jit(solution)/shard_map/ppermute | solution.py:405
  62.0 0.9 slice.59
  62.9 4.6 %collective-permute-start.8 = (bf16[256,1024]{1,0:T(8,128)(2,1)}, bf16[256,1024]{1,0:T(8,128)(2,1)}, u32[]{:S(2)}, u32[]{:S(2)}) collective-permute-start(bf16[256,1024]{1,0:T(8,128)(2,1)} %slice.59), channel_id=1, source_target_pairs={{0,24},{1,7},{2,26},{3,1},{4,28},{5,3},{6,30},{7,5},{8,0},{9,15},{... | collective-permute-start | bytes 1572872 | tf_op jit(solution)/shard_map/ppermute | solution.py:406
  67.5 1.3 constant_dynamic-slice_fusion.floor_ref
  69.4 0.7 constant_dynamic-slice_fusion.1.up_ref
  70.7 0.8 reduce.4
  71.5 0.7 slice.47.rate_ref
  72.2 1.7 collective-permute-done.8.r3b
  73.9 6.4 %project.1 = (bf16[512,768]{1,0:T(8,128)(2,1)}, bf16[512,256]{1,0:T(8,128)(2,1)}) custom-call(s32[20]{0:T(128)} %stack.83.idx_ref, bf16[128,1024]{1,0:T(8,128)(2,1)} %copy-done.6, bf16[128,1024]{1,0:T(8,128)(2,1)} %copy-done.3, bf16[128,1024]{1,0:T(8,128)(2,1)} %copy-done.4, bf16[64,1024]{1,0:T(8,128)(2,1)} %copy-done.8, bf16[64,1024]{1,0:T(8,128)(2,1)} %copy-done.9, ...), custom_call_target="tpu_custom_call" | custom-call | tf_op jit(solution)/shard_map/project/pallas_call | solution.py:345
  80.4 20.1 %prep.1 = (bf16[16,64,128]{2,1,0:T(8,128)(2,1)}, f32[2,512,256]{2,1,0:T(8,128)}, f32[2,512,256]{2,1,0:T(8,128)}) custom-call(bf16[512,768]{1,0:T(8,128)(2,1)} %get-tuple-element.10.q_ref.k_ref.v_ref, bf16[512,768]{1,0:T(8,128)(2,1)} %get-tuple-element.10.q_ref.k_ref.v_ref, bf16[512,768]{1,0:T(8,128)(2,1)} %get-tuple-element.10.q_ref.k_ref.v_ref, ...), custom_call_target="tpu_custom_call" | custom-call | tf_op jit(solution)/shard_map/prep/pallas_call | solution.py:201
  100.5 25.6 %all_to_all.15.u_ref = bf16[16,64,128]{2,1,0:T(8,128)(2,1)} all-to-all(bf16[16,64,128]{2,1,0:T(8,128)(2,1)} %get-tuple-element.14), channel_id=1, replica_groups=mesh['sp'=16,'dp'=32] {'sp'}, dimensions={0} | all-to-all | bytes 524288 | tf_op jit(solution)/shard_map/all_to_all | solution.py:431
  126.1 3.5 %states.1 = bf16[16,32,128]{2,1,0:T(8,128)(2,1)} custom-call(s32[1]{0:T(128)} %bitcast.23.back_ref, bf16[16,64,128]{2,1,0:T(8,128)(2,1)} %all_to_all.15.u_ref), custom_call_target="tpu_custom_call" | custom-call | tf_op jit(solution)/shard_map/states/pallas_call | solution.py:306
  129.6 10.3 %all-to-all-start.2 = ((bf16[16,32,128]{2,1,0:T(8,128)(2,1)}), bf16[16,32,128]{2,1,0:T(8,128)(2,1)S(1)}, u32[]{:S(2)}, u32[]{:S(2)}) async-start(bf16[16,32,128]{2,1,0:T(8,128)(2,1)} %states.1), calls=%async_computation.2 | async-start | bytes 262144 | tf_op jit(solution)/shard_map/all_to_all | solution.py:433
  140.0 0.7 slice.49.diag_ref
  140.6 0.7 slice.51.gain_ref
  141.3 10.6 %all-to-all-done.2.s_ref = bf16[16,32,128]{2,1,0:T(8,128)(2,1)S(1)} async-done(((bf16[16,32,128]{2,1,0:T(8,128)(2,1)}), bf16[16,32,128]{2,1,0:T(8,128)(2,1)S(1)}, u32[]{:S(2)}, u32[]{:S(2)}) %all-to-all-start.2) | async-done | bytes 131104 | tf_op jit(solution)/shard_map/all_to_all | solution.py:433
  151.9 0.6 copy-done.10
  152.6 5.4 %final.1 = bf16[512,256]{1,0:T(8,128)(2,1)} custom-call(f32[2,512,256]{2,1,0:T(8,128)} %get-tuple-element.12.y_ref, f32[2,512,256]{2,1,0:T(8,128)} %get-tuple-element.13.qx_ref, bf16[16,32,128]{2,1,0:T(8,128)(2,1)} %copy-done.10, bf16[512,768]{1,0:T(8,128)(2,1)} %get-tuple-element.10.q_ref.k_ref.v_ref, bf16[512,768]{1,0:T(8,128)(2,1)} %get-tuple-element.10.q_ref.k_ref.v_ref, ...), custom_call_target="tpu_custom_call" | custom-call | tf_op jit(solution)/shard_map/final/pallas_call | solution.py:264
  157.9 1.0 dynamic-slice_bitcast_fusion
  158.9 3.6 %collective-permute-start.12 = (bf16[2,128,256]{2,1,0:T(8,128)(2,1)S(1)}, bf16[2,128,256]{2,1,0:T(8,128)(2,1)S(1)}, u32[]{:S(2)}, u32[]{:S(2)}) collective-permute-start(bf16[2,128,256]{2,1,0:T(8,128)(2,1)S(1)} %dynamic-slice_bitcast_fusion), channel_id=1, source_target_pairs={{0,32},{32,0},{64,96},{96,64},{128,160},{160,128},{192,224},{224,1... | collective-permute-start | bytes 393224 | tf_op jit(solution)/shard_map/ppermute | solution.py:438
  162.6 2.3 %collective-permute-done.12 = bf16[2,128,256]{2,1,0:T(8,128)(2,1)S(1)} collective-permute-done((bf16[2,128,256]{2,1,0:T(8,128)(2,1)S(1)}, bf16[2,128,256]{2,1,0:T(8,128)(2,1)S(1)}, u32[]{:S(2)}, u32[]{:S(2)}) %collective-permute-start.12) | collective-permute-done | bytes 131104 | tf_op jit(solution)/shard_map/ppermute | solution.py:438
  165.0 6.5 %collective-permute-start.13 = (bf16[128,512]{1,0:T(8,128)(2,1)S(1)}, bf16[128,512]{1,0:T(8,128)(2,1)S(1)}, u32[]{:S(2)}, u32[]{:S(2)}) collective-permute-start(bf16[128,512]{1,0:T(8,128)(2,1)S(1)} %fusion.1), channel_id=1, source_target_pairs={{0,1},{1,0},{2,3},{3,2},{4,5},{5,4},{6,7},{7,6},{8,9},{9,8},{10,11... | collective-permute-start | bytes 393224 | tf_op jit(solution)/shard_map/ppermute | solution.py:443
  171.5 1.0 collective-permute-done.13
  172.6 0.7 maximum_bitcast_fusion
  (59 shorter events, 1.9 us)
Async XLA Ops:
  0.0 69.4 %copy-start = (bf16[2,128,1024]{2,1,0:T(8,128)(2,1)S(1)}, bf16[2,128,1024]{2,1,0:T(8,128)(2,1)}, u32[]{:S(2)}) copy-start(bf16[2,128,1024]{2,1,0:T(8,128)(2,1)} %param.15) | copy-start | bytes 1572868
  0.0 1.0 copy-start.12
  1.0 0.8 copy-start.11
  1.8 9.7 %collective-permute-start = (bf16[64,1024]{1,0:T(8,128)(2,1)S(1)}, bf16[64,1024]{1,0:T(8,128)(2,1)S(1)}, u32[]{:S(2)}, u32[]{:S(2)}) collective-permute-start(bf16[64,1024]{1,0:T(8,128)(2,1)S(1)} %pad_maximum_fusion), channel_id=1, source_target_pairs={{0,1},{1,0},{2,3},{3,2},{4,5},{5,4},{6,7},{7,6},{8,9},{9,8},{10,11... | collective-permute-start | bytes 393224 | tf_op jit(solution)/shard_map/ppermute | solution.py:392
  12.3 10.6 %copy-start.6 = (bf16[128,1024]{1,0:T(8,128)(2,1)}, bf16[128,1024]{1,0:T(8,128)(2,1)S(1)}, u32[]{:S(2)}) copy-start(bf16[128,1024]{1,0:T(8,128)(2,1)S(1)} %get-tuple-element.16.b0) | copy-start | bytes 786436
  12.3 8.6 %collective-permute-start.1 = (bf16[128,1024]{1,0:T(8,128)(2,1)S(1)}, bf16[128,1024]{1,0:T(8,128)(2,1)S(1)}, u32[]{:S(2)}, u32[]{:S(2)}) collective-permute-start(bf16[128,1024]{1,0:T(8,128)(2,1)S(1)} %get-tuple-element.16.b0), channel_id=1, source_target_pairs={{0,2},{1,9},{2,4},{3,11},{4,6},{5,13},{6,0},{7,15},{8,10},{9,17},{... | collective-permute-start | bytes 786440 | tf_op jit(solution)/shard_map/ppermute | solution.py:395
  14.2 8.6 %collective-permute-start.2 = (bf16[128,1024]{1,0:T(8,128)(2,1)S(1)}, bf16[128,1024]{1,0:T(8,128)(2,1)S(1)}, u32[]{:S(2)}, u32[]{:S(2)}) collective-permute-start(bf16[128,1024]{1,0:T(8,128)(2,1)S(1)} %get-tuple-element.16.b0), channel_id=1, source_target_pairs={{0,6},{1,25},{2,0},{3,27},{4,2},{5,29},{6,4},{7,31},{8,14},{9,1},{... | collective-permute-start | bytes 786440 | tf_op jit(solution)/shard_map/ppermute | solution.py:396
  20.9 6.6 %copy-start.3 = (bf16[128,1024]{1,0:T(8,128)(2,1)}, bf16[128,1024]{1,0:T(8,128)(2,1)S(1)}, u32[]{:S(2)}) copy-start(bf16[128,1024]{1,0:T(8,128)(2,1)S(1)} %collective-permute-done.1.fm) | copy-start | bytes 786436
  20.9 8.0 %collective-permute-start.3 = (bf16[64,1024]{1,0:T(8,128)(2,1)S(1)}, bf16[64,1024]{1,0:T(8,128)(2,1)S(1)}, u32[]{:S(2)}, u32[]{:S(2)}) collective-permute-start(bf16[64,1024]{1,0:T(8,128)(2,1)S(1)} %slice.56), channel_id=1, source_target_pairs={{0,2},{1,9},{2,4},{3,11},{4,6},{5,13},{6,0},{7,15},{8,10},{9,17},{... | collective-permute-start | bytes 393224 | tf_op jit(solution)/shard_map/ppermute | solution.py:397
  22.9 5.4 %copy-start.4 = (bf16[128,1024]{1,0:T(8,128)(2,1)}, bf16[128,1024]{1,0:T(8,128)(2,1)S(1)}, u32[]{:S(2)}) copy-start(bf16[128,1024]{1,0:T(8,128)(2,1)S(1)} %collective-permute-done.2.fp) | copy-start | bytes 786436
  22.9 6.8 %collective-permute-start.4 = (bf16[64,1024]{1,0:T(8,128)(2,1)S(1)}, bf16[64,1024]{1,0:T(8,128)(2,1)S(1)}, u32[]{:S(2)}, u32[]{:S(2)}) collective-permute-start(bf16[64,1024]{1,0:T(8,128)(2,1)S(1)} %slice.57), channel_id=1, source_target_pairs={{0,6},{1,25},{2,0},{3,27},{4,2},{5,29},{6,4},{7,31},{8,14},{9,1},{... | collective-permute-start | bytes 393224 | tf_op jit(solution)/shard_map/ppermute | solution.py:398
  29.0 0.7 copy-start.8
  29.7 0.7 copy-start.9
  30.3 13.8 %copy-start.14 = (f32[2,64]{1,0:T(2,128)S(1)}, f32[2,64]{1,0:T(2,128)}, u32[]{:S(2)}) copy-start(f32[2,64]{1,0:T(2,128)} %param.17) | copy-start | bytes 1540
  31.0 27.5 %collective-permute-start.5 = (bf16[512,1024]{1,0:T(8,128)(2,1)}, bf16[512,1024]{1,0:T(8,128)(2,1)S(1)}, u32[]{:S(2)}, u32[]{:S(2)}) collective-permute-start(bf16[512,1024]{1,0:T(8,128)(2,1)} %constant_dynamic-update-slice_fusion), channel_id=1, source_target_pairs={{0,8},{1,3},{2,10},{3,5},{4,12},{5,7},{6,14},{7,1},{8,16},{9,11},{... | collective-permute-start | bytes 3145736 | tf_op jit(solution)/shard_map/ppermute | solution.py:402
  32.9 29.1 %collective-permute-start.6 = (bf16[512,1024]{1,0:T(8,128)(2,1)}, bf16[512,1024]{1,0:T(8,128)(2,1)S(1)}, u32[]{:S(2)}, u32[]{:S(2)}) collective-permute-start(bf16[512,1024]{1,0:T(8,128)(2,1)} %constant_dynamic-update-slice_fusion), channel_id=1, source_target_pairs={{0,24},{1,7},{2,26},{3,1},{4,28},{5,3},{6,30},{7,5},{8,0},{9,15},{... | collective-permute-start | bytes 3145736 | tf_op jit(solution)/shard_map/ppermute | solution.py:403
  37.5 18.7 %collective-permute-start.9 = (bf16[128,2048]{1,0:T(8,128)(2,1)}, bf16[128,2048]{1,0:T(8,128)(2,1)S(1)}, u32[]{:S(2)}, u32[]{:S(2)}) collective-permute-start(bf16[128,2048]{1,0:T(8,128)(2,1)} %bitcast.20.t0), channel_id=1, source_target_pairs={{0,32},{32,0},{64,96},{96,64},{128,160},{160,128},{192,224},{224,1... | collective-permute-start | bytes 1572872 | tf_op jit(solution)/shard_map/ppermute | solution.py:399
  39.4 32.8 %collective-permute-start.10 = (bf16[128,2048]{1,0:T(8,128)(2,1)}, bf16[128,2048]{1,0:T(8,128)(2,1)}, u32[]{:S(2)}, u32[]{:S(2)}) collective-permute-start(bf16[128,2048]{1,0:T(8,128)(2,1)} %bitcast.20.t0), channel_id=1, source_target_pairs={{0,1},{1,0},{2,3},{3,2},{4,5},{5,4},{6,7},{7,6},{8,9},{9,8},{10,11... | collective-permute-start | bytes 1572872 | tf_op jit(solution)/shard_map/ppermute | solution.py:400
  44.1 0.7 copy-start.13
  44.1 0.7 copy-start.15
  45.5 24.6 %all-to-all-start = ((f32[16,1,512]{2,1,0:T(1,128)}), f32[16,1,512]{2,1,0:T(1,128)S(1)}, u32[]{:S(2)}, u32[]{:S(2)}) async-start(f32[16,1,512]{2,1,0:T(1,128)} %reshape.28), calls=%async_computation | async-start | bytes 65536 | tf_op jit(solution)/shard_map/all_to_all | solution.py:410
  56.2 6.7 %copy-start.7 = (bf16[128,2048]{1,0:T(8,128)(2,1)}, bf16[128,2048]{1,0:T(8,128)(2,1)S(1)}, u32[]{:S(2)}) copy-start(bf16[128,2048]{1,0:T(8,128)(2,1)S(1)} %collective-permute-done.9.t1) | copy-start | bytes 1572868
  56.2 16.0 %collective-permute-start.11 = (bf16[128,2048]{1,0:T(8,128)(2,1)S(1)}, bf16[128,2048]{1,0:T(8,128)(2,1)}, u32[]{:S(2)}, u32[]{:S(2)}) collective-permute-start(bf16[128,2048]{1,0:T(8,128)(2,1)S(1)} %collective-permute-done.9.t1), channel_id=1, source_target_pairs={{0,1},{1,0},{2,3},{3,2},{4,5},{5,4},{6,7},{7,6},{8,9},{9,8},{10,11... | collective-permute-start | bytes 1572872 | tf_op jit(solution)/shard_map/ppermute | solution.py:404
  58.5 10.3 %copy-start.1 = (bf16[512,1024]{1,0:T(8,128)(2,1)}, bf16[512,1024]{1,0:T(8,128)(2,1)S(1)}, u32[]{:S(2)}) copy-start(bf16[512,1024]{1,0:T(8,128)(2,1)S(1)} %collective-permute-done.5.r1) | copy-start | bytes 3145732
  59.4 12.8 %collective-permute-start.7 = (bf16[256,1024]{1,0:T(8,128)(2,1)}, bf16[256,1024]{1,0:T(8,128)(2,1)}, u32[]{:S(2)}, u32[]{:S(2)}) collective-permute-start(bf16[256,1024]{1,0:T(8,128)(2,1)} %slice.58), channel_id=1, source_target_pairs={{0,8},{1,3},{2,10},{3,5},{4,12},{5,7},{6,14},{7,1},{8,16},{9,11},{... | collective-permute-start | bytes 1572872 | tf_op jit(solution)/shard_map/ppermute | solution.py:405
  62.0 11.9 %copy-start.2 = (bf16[512,1024]{1,0:T(8,128)(2,1)}, bf16[512,1024]{1,0:T(8,128)(2,1)S(1)}, u32[]{:S(2)}) copy-start(bf16[512,1024]{1,0:T(8,128)(2,1)S(1)} %collective-permute-done.6.r2) | copy-start | bytes 3145732
  62.9 11.0 %collective-permute-start.8 = (bf16[256,1024]{1,0:T(8,128)(2,1)}, bf16[256,1024]{1,0:T(8,128)(2,1)}, u32[]{:S(2)}, u32[]{:S(2)}) collective-permute-start(bf16[256,1024]{1,0:T(8,128)(2,1)} %slice.59), channel_id=1, source_target_pairs={{0,24},{1,7},{2,26},{3,1},{4,28},{5,3},{6,30},{7,5},{8,0},{9,15},{... | collective-permute-start | bytes 1572872 | tf_op jit(solution)/shard_map/ppermute | solution.py:406
  129.6 22.3 %all-to-all-start.2 = ((bf16[16,32,128]{2,1,0:T(8,128)(2,1)}), bf16[16,32,128]{2,1,0:T(8,128)(2,1)S(1)}, u32[]{:S(2)}, u32[]{:S(2)}) async-start(bf16[16,32,128]{2,1,0:T(8,128)(2,1)} %states.1), calls=%async_computation.2 | async-start | bytes 262144 | tf_op jit(solution)/shard_map/all_to_all | solution.py:433
  151.9 0.6 copy-start.10
  157.9 7.0 %copy-start.5 = (bf16[512,256]{1,0:T(8,128)(2,1)S(1)}, bf16[512,256]{1,0:T(8,128)(2,1)}, u32[]{:S(2)}) copy-start(bf16[512,256]{1,0:T(8,128)(2,1)} %final.1) | copy-start | bytes 786436
  158.9 6.0 %collective-permute-start.12 = (bf16[2,128,256]{2,1,0:T(8,128)(2,1)S(1)}, bf16[2,128,256]{2,1,0:T(8,128)(2,1)S(1)}, u32[]{:S(2)}, u32[]{:S(2)}) collective-permute-start(bf16[2,128,256]{2,1,0:T(8,128)(2,1)S(1)} %dynamic-slice_bitcast_fusion), channel_id=1, source_target_pairs={{0,32},{32,0},{64,96},{96,64},{128,160},{160,128},{192,224},{224,1... | collective-permute-start | bytes 393224 | tf_op jit(solution)/shard_map/ppermute | solution.py:438
  165.0 7.5 %collective-permute-start.13 = (bf16[128,512]{1,0:T(8,128)(2,1)S(1)}, bf16[128,512]{1,0:T(8,128)(2,1)S(1)}, u32[]{:S(2)}, u32[]{:S(2)}) collective-permute-start(bf16[128,512]{1,0:T(8,128)(2,1)S(1)} %fusion.1), channel_id=1, source_target_pairs={{0,1},{1,0},{2,3},{3,2},{4,5},{5,4},{6,7},{7,6},{8,9},{9,8},{10,11... | collective-permute-start | bytes 393224 | tf_op jit(solution)/shard_map/ppermute | solution.py:443

commit v2 on v1

v2 whole, which is shorter than its diff:
```python
import math
import functools
import jax
import jax.numpy as jnp
from jax import lax
from jax.experimental import pallas as pl
from jax.experimental.pallas import tpu as pltpu
from jax.sharding import PartitionSpec as P

BF = jnp.bfloat16
F32 = jnp.float32
C = 128
H = 64


def split2(x):
    hi = x.astype(BF)
    return hi, (x - hi.astype(F32)).astype(BF)


def left3(a):
    hi, lo = split2(a)
    return jnp.concatenate([hi, lo], 1)


def right3(b):
    hi, lo = split2(b)
    return jnp.concatenate(
        [jnp.concatenate([hi, lo], 1), jnp.concatenate([hi, jnp.zeros_like(lo)], 1)], 0
    )


def dot3(a3, b3):
    t = jnp.dot(a3, b3, preferred_element_type=F32)
    n = t.shape[1] // 2
    return t[:, :n] + t[:, n:]


def nt(a, b):
    return lax.dot_general(a, b, (((1,), (1,)), ((), ())), preferred_element_type=F32)


def tn(a, b):
    return lax.dot_general(a, b, (((0,), (0,)), ((), ())), preferred_element_type=F32)


def head_ones(scale=1.0):
    r = lax.broadcasted_iota(jnp.int32, (256, 128), 0)
    c = lax.broadcasted_iota(jnp.int32, (256, 128), 1)
    return jnp.where(((r >> 6) & 1) == (c >> 6), scale, 0.0).astype(BF)


def head_sum(x, ones):
    hi, lo = split2(x)
    return jnp.dot(jnp.concatenate([hi, lo], 1), ones, preferred_element_type=F32)


def mm(a, b):
    return jnp.dot(a.astype(BF), b.astype(BF), preferred_element_type=F32)


def product(a, b):
    return dot3(left3(a), right3(b))


def pick_rows(x, size, off):
    return jnp.concatenate([x[i + off : i + off + size] for i in range(0, C, 2 * size)], 0)


def put_rows(rows, rest, size, off):
    parts = []
    for n, i in enumerate(range(0, C, 2 * size)):
        new = rows[n * size : (n + 1) * size]
        old = rest[i : i + size] if off else rest[i + size : i + 2 * size]
        parts += [old, new] if off else [new, old]
    return jnp.concatenate(parts, 0)


def gates(d, low, up, floor, pair):
    lanes = pl.ds(pl.multiple_of(pair * 128, 128), 128)
    pre = (
        jnp.dot(low[:, d * 128 : (d + 1) * 128], up[d, :, lanes], preferred_element_type=F32)
        + floor[d : d + 1, lanes]
    )
    return -math.exp(-0.5) * jax.nn.sigmoid(pre.astype(BF).astype(F32))


def head_row(par, pair, i):
    return jnp.concatenate([par[2 * pair, i : i + 1, :], par[2 * pair + 1, i : i + 1, :]], 1)


def sums(d, ld, tri):
    hi, lo = split2(ld)
    cs = jnp.dot(tri, jnp.concatenate([hi, lo], 1), preferred_element_type=F32)
    inc = cs[:, :128] + cs[:, 128:]
    return inc, inc[C // 2 : C // 2 + 1], inc[C - 1 : C] if d == 0 else inc[0:1]


def against(parts, pk):
    pkh, pkl = split2(pk)
    rhs = jnp.concatenate(
        [jnp.concatenate([pkh, pkh], 1), jnp.concatenate([pkl, jnp.zeros_like(pkl)], 1)], 0
    )
    att = nt(jnp.concatenate([left3(p) for p in parts], 0), rhs)
    att = att[:, :C] + att[:, C:]
    return [att[i * C : (i + 1) * C] for i in range(len(parts))]


def consts():
    row = lax.broadcasted_iota(jnp.int32, (C, C), 0)
    col = lax.broadcasted_iota(jnp.int32, (C, C), 1)
    tris = [jnp.where(m, 1.0, 0.0).astype(BF) for m in (col <= row, col >= row)]
    return row, col, row ^ col, col < H, tris


def maps_kernel(role, k_ref, v_ref, low_ref, up_ref, floor_ref, par_ref, msg_ref, x_ref, u_ref):
    chunks = k_ref.shape[0] // C
    row, col, x, left, tris = consts()
    hps = k_ref.shape[1] // 128
    probs = []
    for hp, d in [(hp, d) for hp in range(hps) for d in range(2)]:
        ln = slice(hp * 128, (hp + 1) * 128)
        k = k_ref[:, ln].astype(F32)
        v = v_ref[:, ln].astype(F32)
        nk = -(k / (1.0 + head_sum(k * k, head_ones())))
        pair = role() * hps + hp
        logd = gates(d, low_ref, up_ref, floor_ref, pair)
        kap = k * jax.nn.sigmoid(head_row(par_ref, pair, d))
        strict = (col < row) if d == 0 else (col > row)
        for ci in range(chunks):
            c = ci if d == 0 else chunks - 1 - ci
            sl = slice(c * C, (c + 1) * C)
            ld = logd[sl]
            inc, mid, fin = sums(d, ld, tris[d])
            rel = inc - mid
            gq = nk[sl] * jnp.exp(rel - ld)
            pk = kap[sl] * jnp.exp(-rel)
            ke = pk * jnp.exp(fin - mid)
            gl = pltpu.roll(gq * jnp.exp(mid), H, 1)
            vs = v[sl]
            zero = jnp.zeros_like(gq)
            att = against([jnp.where(left, gq, zero), jnp.where(left, zero, gq)], pk)
            heads = []
            for a in range(2):
                m = jnp.where(strict, att[a], 0.0)
                b = jnp.where(left, vs, gl) if a == 0 else jnp.where(left, gl, vs)
                heads.append(dict(m=m, b=b, d=d))
            probs.append(dict(d=d, c=c, heads=heads, ke=ke, fin=fin))
    allh = [h for p in probs for h in p["heads"]]
    zero = jnp.zeros((C, C), F32)
    for h in allh:
        h["n"] = jnp.where(x == 1, h["m"], 0.0)
    for lb in range(1, 7):
        size = 1 << lb
        sel = (x >> lb) == 1
        for h in allh:
            off = jnp.where(sel, h["m"], 0.0)
            if size >= 8:
                at = size if h["d"] == 0 else 0
                off = pick_rows(off, size, at)
                h["w"] = off + mm(off, h["n"])
            else:
                h["w"] = off + mm(off, h["n"])
        for h in allh:
            if size >= 8:
                at = size if h["d"] == 0 else 0
                nr = pick_rows(h["n"], size, at)
                nr = nr + h["w"] + mm(nr, put_rows(h["w"], zero, size, at))
                h["n"] = put_rows(nr, h["n"], size, at)
            else:
                h["n"] = h["n"] + h["w"] + mm(h["n"], h["w"])
    for h in allh:
        h["nb"] = h["n"].astype(BF)
        h["x"] = h["b"] + mm(h["nb"], h["b"])
    for h in allh:
        h["res"] = h["b"] - h["x"] + product(h["m"], h["x"])
    for h in allh:
        h["x"] = h["x"] + h["res"] + mm(h["nb"], h["res"])
    for hp, d in [(hp, d) for hp in range(hps) for d in range(2)]:
        u = None
        for ci in range(chunks):
            p = probs[(hp * 2 + d) * chunks + ci]
            xa, xb = p["heads"][0]["x"], p["heads"][1]["x"]
            x_ref[hp, d, p["c"], 0] = xa
            x_ref[hp, d, p["c"], 1] = xb
            kh, kl = split2(
                jnp.concatenate([jnp.where(left, p["ke"], 0.0), jnp.where(left, 0.0, p["ke"])], 0)
            )
            xh, xl = split2(jnp.concatenate([xa, xb], 0))
            un = tn(kh, jnp.concatenate([xh, xl], 1))
            un = un[:, :C] + un[:, C:] + tn(kl, xh)
            un = jnp.where(row < H, un, pltpu.roll(un, H, 1))
            ef = jnp.broadcast_to(jnp.exp(p["fin"]), (C, C))
            dm = jnp.where(row < H, pltpu.roll(ef, H, 1), ef)
            un = un + jnp.where(col == (row & (H - 1)) + H, dm, 0.0)
            if u is None:
                u = un
                u_ref[hp, d] = u
            else:
                t2 = jnp.where(
                    row < H,
                    jnp.where(left, pltpu.roll(un, H, 1), 0.0),
                    jnp.where(left, 0.0, un),
                )
                u = product(t2, u) + jnp.where(left, un, 0.0)
        msg_ref[4 * hp + d] = u[:H].astype(BF)
        msg_ref[4 * hp + 2 + d] = u[H:].astype(BF)


def outputs_kernel(
    role, q_ref, k_ref, v_ref, low_ref, up_ref, floor_ref, par_ref, x_ref, u_ref, y_ref, qx_ref, own_ref
):
    chunks = k_ref.shape[0] // C
    q = q_ref[...].astype(F32)
    k = k_ref[...].astype(F32)
    row, _, _, left, tris = consts()
    pair = role() * pl.num_programs(1) + pl.program_id(1)
    rates = [jax.nn.sigmoid(head_row(par_ref, pair, d)) for d in range(2)]
    wt = rates[0] * head_row(par_ref, pair, 2) + rates[1] * head_row(par_ref, pair, 3)
    own_ref[...] = head_sum(q * k * wt, head_ones()) * v_ref[...].astype(F32)
    for d in range(2):
        logd = gates(d, low_ref, up_ref, floor_ref, pair)
        kap = k * rates[d]
        u = u_ref[0, d]
        for ci in range(chunks):
            c = ci if d == 0 else chunks - 1 - ci
            sl = slice(c * C, (c + 1) * C)
            inc, mid, _ = sums(d, logd[sl], tris[d])
            rel = inc - mid
            rq = q[sl] * jnp.exp(rel)
            pk = kap[sl] * jnp.exp(-rel)
            zero = jnp.zeros_like(rq)
            att = against([jnp.where(left, rq, zero), jnp.where(left, zero, rq)], pk)
            ya, yb = [
                product(jnp.where(tris[d] > 0, att[a], 0.0), x_ref[0, d, c, a]) for a in range(2)
            ]
            y0 = jnp.where(left, ya, yb)
            qx = rq * jnp.exp(mid) + pltpu.roll(jnp.where(left, yb, ya), H, 1)
            if ci > 0:
                up_i = jnp.where(left, u, 0.0)
                ub_i = jnp.where(row < H, up_i, pltpu.roll(up_i, H, 1))
                up_t = jnp.where(left, 0.0, u)
                ub_t = jnp.where(row < H, pltpu.roll(up_t, H, 1), up_t)
                bh, bl = split2(jnp.concatenate([ub_i, ub_t], 1))
                q3 = left3(qx)
                qd = jnp.dot(
                    q3, jnp.concatenate([bh, bh], 0), preferred_element_type=F32
                ) + jnp.dot(q3[:, :C], bl, preferred_element_type=F32)
                y0 = y0 + qd[:, :C]
                qx = qd[:, C:]
            y_ref[d, sl, :] = y0
            qx_ref[d, sl, :] = qx


def layout(qkv, tokens):
    rows, width3 = qkv.shape
    width = width3 // 3
    seqs, hps, chunks = rows // tokens, width // 128, tokens // C
    part = lambda off: pl.BlockSpec((tokens, 128), lambda s, h: (s, h + off * hps))
    specs = dict(
        q=part(0),
        k=part(1),
        v=part(2),
        low=pl.BlockSpec((tokens, 256), lambda s, h: (s, 0)),
        x=pl.BlockSpec((1, 2, chunks, 2, C, 128), lambda s, h: (s * hps + h, 0, 0, 0, 0, 0)),
        u=pl.BlockSpec((1, 2, C, 128), lambda s, h: (s * hps + h, 0, 0, 0)),
        y=pl.BlockSpec((2, tokens, 128), lambda s, h: (0, s, h)),
        out=part(0),
    )
    return rows, width, seqs, hps, chunks, specs


def whole(*arrays):
    return [pl.BlockSpec(a.shape, lambda *i, n=a.ndim: (0,) * n) for a in arrays]


BIG = pltpu.CompilerParams(vmem_limit_bytes=56 * 1024 * 1024)


def maps(role, qkv, low, up, floor, par, tokens):
    _, width, seqs, hps, chunks, _ = layout(qkv, tokens)
    return pl.pallas_call(
        functools.partial(maps_kernel, role),
        grid=(seqs,),
        in_specs=[
            pl.BlockSpec((tokens, width), lambda s: (s, 1)),
            pl.BlockSpec((tokens, width), lambda s: (s, 2)),
            pl.BlockSpec((tokens, 256), lambda s: (s, 0)),
            *whole(up, floor, par),
        ],
        out_specs=[
            pl.BlockSpec((4 * hps, H, 128), lambda s: (s, 0, 0)),
            pl.BlockSpec((hps, 2, chunks, 2, C, 128), lambda s: (s, 0, 0, 0, 0, 0)),
            pl.BlockSpec((hps, 2, C, 128), lambda s: (s, 0, 0, 0)),
        ],
        out_shape=[
            jax.ShapeDtypeStruct((seqs * hps * 4, H, 128), BF),
            jax.ShapeDtypeStruct((seqs * hps, 2, chunks, 2, C, 128), F32),
            jax.ShapeDtypeStruct((seqs * hps, 2, C, 128), F32),
        ],
        compiler_params=BIG,
        cost_estimate=pl.CostEstimate(flops=8_000_000_000, bytes_accessed=6_000_000, transcendentals=0),
        name="maps",
    )(qkv, qkv, low, up, floor, par)


def outputs(role, qkv, low, up, floor, par, x, u, tokens):
    rows, width, seqs, hps, _, sp = layout(qkv, tokens)
    return pl.pallas_call(
        functools.partial(outputs_kernel, role),
        grid=(seqs, hps),
        in_specs=[
            sp["q"], sp["k"], sp["v"], sp["low"], *whole(up, floor, par), sp["x"], sp["u"]
        ],
        out_specs=[sp["y"], sp["y"], sp["out"]],
        out_shape=[
            jax.ShapeDtypeStruct((2, rows, width), F32),
            jax.ShapeDtypeStruct((2, rows, width), F32),
            jax.ShapeDtypeStruct((rows, width), F32),
        ],
        compiler_params=BIG,
        cost_estimate=pl.CostEstimate(flops=4_000_000_000, bytes_accessed=8_000_000, transcendentals=0),
        name="outputs",
    )(qkv, qkv, qkv, low, up, floor, par, x, u)


def final_kernel(role, y_ref, qx_ref, s_ref, own_ref, par_ref, o_ref):
    mean = head_ones(1.0 / H)
    z = jnp.zeros((H, H), BF)
    hps = own_ref.shape[1] // 128
    for hp in range(hps):
        ln = slice(hp * 128, (hp + 1) * 128)
        total = own_ref[:, ln]
        gain = head_row(par_ref, role() * hps + hp, 4)
        for d in range(2):
            sa, sb = s_ref[4 * hp + d], s_ref[4 * hp + 2 + d]
            blk = jnp.concatenate(
                [
                    jnp.concatenate([jnp.concatenate([sa[:, :H], sa[:, H:]], 0), z], 1),
                    jnp.concatenate([z, jnp.concatenate([sb[:, :H], sb[:, H:]], 0)], 1),
                ],
                0,
            )
            y = y_ref[d, :, ln] + jnp.dot(
                left3(qx_ref[d, :, ln]), jnp.concatenate([blk, blk], 0), preferred_element_type=F32
            )
            cen = y - head_sum(y, mean)
            var = head_sum(cen * cen, mean)
            total = total + cen * lax.rsqrt(var + 0.00064) * gain
        o_ref[:, ln] = total.astype(BF)


def final(role, y, qx, s, own, par, tokens):
    rows, width = own.shape
    hps = width // 128
    dspec = pl.BlockSpec((2, tokens, width), lambda s: (0, s, 0))
    one = pl.BlockSpec((tokens, width), lambda s: (s, 0))
    return pl.pallas_call(
        functools.partial(final_kernel, role),
        grid=(rows // tokens,),
        in_specs=[
            dspec,
            dspec,
            pl.BlockSpec((4 * hps, 32, 128), lambda s: (s, 0, 0)),
            one,
            *whole(par),
        ],
        out_specs=one,
        out_shape=jax.ShapeDtypeStruct((rows, width), BF),
        compiler_params=BIG,
        name="final",
    )(y, qx, s, own, par)


def scan_kernel(roles, back_of, u_ref, o_ref):
    groups = u_ref.shape[0] // roles
    back = back_of()
    states = [jnp.zeros((H, H), F32) for _ in range(roles)]
    zero = jnp.zeros((H, 128), BF)
    for i in range(groups):
        g = jnp.where(back == 1, groups - 1 - i, i)
        for p in range(roles):
            src = g * roles + p
            s = states[p]
            hi, lo = split2(s)
            o_ref[src] = jnp.concatenate([hi[:32], hi[32:]], 1)
            u = u_ref[src]
            t = jnp.dot(
                u, jnp.concatenate([zero, jnp.concatenate([hi, lo], 1)], 0), preferred_element_type=F32
            )
            states[p] = u[:, :H].astype(F32) + t[:, :H] + t[:, H:]


def scan_states(u, back, roles):
    n = u.shape[0]
    return pl.pallas_call(
        functools.partial(scan_kernel, roles, back),
        in_specs=[pl.BlockSpec(memory_space=pltpu.VMEM)],
        out_specs=pl.BlockSpec(memory_space=pltpu.VMEM),
        out_shape=jax.ShapeDtypeStruct((n, 32, 128), BF),
        name="states",
    )(u)


def place():
    z, dp = lax.axis_index("sp"), lax.axis_index("dp")
    j = dp // 2
    return z % 2, dp % 2, j // 4, j % 4


def role():
    p, c, _, _ = place()
    return 2 * p + c


def backwards():
    return lax.axis_index("sp") % 2


def project_kernel(b0, fm, fp, fo, r1, r2, r3t, r3b, t0, t1, t2, t3, qkv_ref, low_ref, w_ref, t_ref, sem):
    p, c, y, x = place()
    rows = b0.shape[0]
    n = t0.shape[0]
    a = jnp.where(c == 0, x, y)
    b = jnp.where(c == 0, y, x)
    copies = []

    def move(src, dst):
        cp = pltpu.make_async_copy(src, dst, sem.at[len(copies)])
        cp.start()
        copies.append(cp)

    for i, t in enumerate((t0, t1, t2, t3)):
        at = 2 * (c if i < 2 else 1 - c) + (p if i % 2 == 0 else 1 - p)
        move(t, t_ref.at[pl.ds(pl.multiple_of(at * n, n), n)])
    for eps, parts in (
        (0, [(b0, 0), (fm, 0), (fp, 0), (fo, 0)]),
        (-1, [(r1, i) for i in range(4)]),
        (1, [(r2, i) for i in range(4)]),
        (2, [(r3t, 0), (r3t, 1), (r3b, 0), (r3b, 1)]),
    ):
        for delta, (ref, i) in zip((0, -1, 1, 2), parts):
            aa, bb = lax.rem(a + delta + 4, 4), lax.rem(b + eps + 4, 4)
            chip = jnp.where(c == 0, bb * 4 + aa, aa * 4 + bb)
            move(ref.at[pl.ds(i * rows, rows)], w_ref.at[chip])
    for cp in copies:
        cp.wait()
    width3 = qkv_ref.shape[1]
    out = jnp.dot(t_ref[...], w_ref[...].reshape(-1, w_ref.shape[2]), preferred_element_type=F32)
    qkv_ref[...] = out[:, :width3].astype(BF)
    low_ref[...] = jnp.tanh(out[:, width3:]).astype(BF)


def project(blocks, toks, width3):
    rows, cols = blocks[0].shape
    n, depth = toks[0].shape
    vm = pl.BlockSpec(memory_space=pltpu.VMEM)
    return pl.pallas_call(
        project_kernel,
        in_specs=[pl.BlockSpec(memory_space=pl.ANY)] * 12,
        out_specs=[vm, vm],
        out_shape=[
            jax.ShapeDtypeStruct((4 * n, width3), BF),
            jax.ShapeDtypeStruct((4 * n, cols - width3), BF),
        ],
        scratch_shapes=[
            pltpu.VMEM((16, rows, cols), BF),
            pltpu.VMEM((4 * n, depth), BF),
            pltpu.SemaphoreType.DMA((20,)),
        ],
        compiler_params=BIG,
        name="project",
    )(*blocks, *toks)


def shift(first, by):
    pairs = []
    for i in range(32):
        core, j = i % 2, i // 2
        y, x = j // 4, j % 4
        if (core == 0) == first:
            x = (x + by) % 4
        else:
            y = (y + by) % 4
        pairs.append((i, (y * 4 + x) * 2 + core))
    return pairs


CORES = [(i, i ^ 1) for i in range(32)]
ZPAIRS = [(i, i ^ 1) for i in range(16)]


def body(tokens, wq, wk, wv, wd, up, floor, rate, diag, gain):
    p, c, _, _ = place()
    width = 256
    tok = tokens.reshape(-1, tokens.shape[2])
    n = tok.shape[0]

    def columns(r):
        cut = lambda w: lax.dynamic_slice_in_dim(w, r * width, width, 1)
        return jnp.concatenate([cut(wq), cut(wk), cut(wv), wd], 1)

    keep = columns(2 * p + c)
    recv = lax.ppermute(columns(2 * p + 1 - c), "dp", CORES)
    b0 = jnp.where(c == 0, jnp.concatenate([keep, recv], 0), jnp.concatenate([recv, keep], 0))
    rows = b0.shape[0]
    fm = lax.ppermute(b0, "dp", shift(True, 1))
    fp = lax.ppermute(b0, "dp", shift(True, -1))
    fo = lax.ppermute(b0, "dp", shift(True, 2))
    tz = lax.ppermute(tok, "sp", ZPAIRS)
    tc = lax.ppermute(tok, "dp", CORES)
    s4 = jnp.concatenate([b0, fm, fp, fo], 0)

    par = jnp.concatenate([rate, diag, gain[None], jnp.zeros((3, gain.shape[0]), F32)], 0)
    par = jnp.broadcast_to(par[None], (16,) + par.shape)
    par = lax.all_to_all(par, "sp", split_axis=0, concat_axis=0, tiled=True)
    r1 = lax.ppermute(s4, "dp", shift(False, 1))
    r2 = lax.ppermute(s4, "dp", shift(False, -1))
    tcz = lax.ppermute(tz, "dp", CORES)
    r3t = lax.ppermute(r1[: 2 * rows], "dp", shift(False, 1))
    r3b = lax.ppermute(r2[2 * rows :], "dp", shift(False, -1))
    qkv, low = project((b0, fm, fp, fo, r1, r2, r3t, r3b), (tok, tz, tc, tcz), 3 * width)
    span = 2 * n
    msg, xs, us = maps(role, qkv, low, up, floor, par, span)
    got = lax.all_to_all(msg, "sp", split_axis=0, concat_axis=0, tiled=True)
    y0, qx, own = outputs(role, qkv, low, up, floor, par, xs, us, span)
    st = scan_states(got, backwards, 2)
    st = lax.all_to_all(st, "sp", split_axis=0, concat_axis=0, tiled=True)
    out = final(role, y0, qx, st, own, par, span)

    out = out.reshape(2, 2, n, width)
    mine = lax.dynamic_index_in_dim(out, p, 1, False)
    rz = lax.ppermute(lax.dynamic_index_in_dim(out, 1 - p, 1, False), "sp", ZPAIRS)
    pick = lambda m, s: lax.dynamic_index_in_dim(m, s, 0, False)
    low_p = jnp.where(p == 0, mine, rz)
    high_p = jnp.where(p == 0, rz, mine)
    both = jnp.concatenate([low_p, high_p], 2)
    far = lax.ppermute(pick(both, 1 - c), "dp", CORES)
    near = pick(both, c)
    first = jnp.where(c == 0, near, far)
    second = jnp.where(c == 0, far, near)
    res = jnp.concatenate(
        [first[:, :width], second[:, :width], first[:, width:], second[:, width:]], 1
    )
    return res.reshape(1, n, 4 * width)


def solution(mesh):
    in_specs = (
        P("dp", "sp", None),
        P("dp", None),
        P("dp", None),
        P("dp", None),
        P("dp", None),
        P(),
        P(),
        P(None, "sp"),
        P(None, "sp"),
        P("sp"),
    )
    return jax.shard_map(
        body, mesh=mesh, in_specs=in_specs, out_specs=P("dp", "sp", None), check_vma=False
    )
```

time: 174 us -> 168 us (0.966)
  starting transfers between devices: 75.1 us -> 62 us
  blocking collectives: 25.6 us -> 37.9 us
  local copies, waits for them, and re-layouts: 15.5 us -> 4.7 us
  Pallas kernels: 35.4 us -> 38.8 us
  other arithmetic: 2.43 us -> 4.23 us
    all_to_all x0 -> x1, blocking collectives: none -> 20.9 us  [body(): par = lax.all_to_all(par, 'sp', split_axis=0, concat_axis=0, tiled=True)]
    all_to_all x1 -> x0, starting transfers between devices: 10.6 us -> none  [body(): par = lax.all_to_all(par, 'sp', split_axis=0, concat_axis=0, tiled=True)]
    all_to_all x1, waiting for transfers between devices: 10.6 us -> 0.37 us  [body(): st = lax.all_to_all(st, 'sp', split_axis=0, concat_axis=0, tiled=True)]
    all_to_all x1, blocking collectives: 25.6 us -> 16.9 us  [body(): got = lax.all_to_all(msg, 'sp', split_axis=0, concat_axis=0, tiled=True)]
    ppermute x1, waiting for transfers between devices: 0.01 us -> 7.02 us  [body(): tz = lax.ppermute(tok, 'sp', ZPAIRS)]
    ppermute x2 -> x1, starting transfers between devices: 6.49 us -> 1.92 us  [body(): fo = lax.ppermute(b0, 'dp', shift(True, 2))]
    ppermute x1, waiting for transfers between devices: 0.01 us -> 3.99 us  [body(): fp = lax.ppermute(b0, 'dp', shift(True, -1))]
    unnamed x37 -> x22, local copies, waits for them, and re-layouts: 5.1 us -> 1.48 us
  transfers between devices with their start and end apart: 16 -> 14, of which waited for: 6 -> 8; matrix products, arithmetic and copies ran while one was open for 6% -> 1% of each run, Pallas kernels for 0% -> 7%
where the time goes in v2:
time: 168 us; the launch traced here: 167 us
  starting transfers between devices  62 us (37%)
  Pallas kernels  38.8 us (23%)
  blocking collectives  37.9 us (23%)
  waiting for transfers between devices  19 us (11%)
  local copies, waits for them, and re-layouts  4.7 us (3%)
  other arithmetic  4.23 us (3%)
    all_to_all x1, blocking collectives, body(): par = lax.all_to_all(par, 'sp', split_axis=0, concat_axis=0, tiled=True)  20.9 us
    all_to_all x1, blocking collectives, body(): got = lax.all_to_all(msg, 'sp', split_axis=0, concat_axis=0, tiled=True)  16.9 us
    pallas_call x1, Pallas kernels, maps(): pl.pallas_call(functools.partial(maps_kernel, role), grid=(seqs,), in_spe...  13.1 us
    pallas_call x1, Pallas kernels, outputs(): pl.pallas_call(functools.partial(outputs_kernel, role), grid=(seqs, hps),...  11.6 us
    all_to_all x1, starting transfers between devices, body(): st = lax.all_to_all(st, 'sp', split_axis=0, concat_axis=0, tiled=True)  10.3 us
    ppermute x1, starting transfers between devices, body(): recv = lax.ppermute(columns(2 * p + 1 - c), 'dp', CORES)  8.75 us
    ppermute x1, starting transfers between devices, body(): far = lax.ppermute(pick(both, 1 - c), 'dp', CORES)  7.09 us
    ppermute x1, waiting for transfers between devices, body(): tz = lax.ppermute(tok, 'sp', ZPAIRS)  7.02 us
  transfers between devices with their start and end apart: 14, of which 8 were waited for; matrix products, arithmetic and copies ran while one was open for 1% of the time, Pallas kernels for 7%

profile of v2, /device:TPU:1, one launch (start us, length us, event | category | flops | bytes accessed | tf_op | source)
XLA Modules:
  0.0 167.0 jit_solution(15181955502383351633)
XLA Ops:
  0.0 0.8 constant_dynamic-slice_fusion.5
  0.8 0.8 constant_dynamic-slice_fusion.3
  1.6 0.8 pad_maximum_fusion.1
  2.4 8.7 %collective-permute-start = (bf16[64,1024]{1,0:T(8,128)(2,1)S(1)}, bf16[64,1024]{1,0:T(8,128)(2,1)S(1)}, u32[]{:S(2)}, u32[]{:S(2)}) collective-permute-start(bf16[64,1024]{1,0:T(8,128)(2,1)S(1)} %pad_maximum_fusion.1), channel_id=1, source_target_pairs={{0,1},{1,0},{2,3},{3,2},{4,5},{5,4},{6,7},{7,6},{8,9},{9,8},{10,11... | collective-permute-start | bytes 393224 | tf_op jit(solution)/shard_map/ppermute | solution.py:504
  11.1 1.0 collective-permute-done
  12.1 0.9 maximum_select_fusion.b0
  13.0 0.0 copy-start
  13.0 0.0 copy-start.7
  13.0 0.0 copy-start.8
  13.0 2.1 %collective-permute-start.1 = (bf16[128,1024]{1,0:T(8,128)(2,1)S(1)}, bf16[128,1024]{1,0:T(8,128)(2,1)S(1)}, u32[]{:S(2)}, u32[]{:S(2)}) collective-permute-start(bf16[128,1024]{1,0:T(8,128)(2,1)S(1)} %maximum_select_fusion.b0), channel_id=1, source_target_pairs={{0,2},{1,9},{2,4},{3,11},{4,6},{5,13},{6,0},{7,15},{8,10},{9,17},{... | collective-permute-start | bytes 786440 | tf_op jit(solution)/shard_map/ppermute | solution.py:507
  15.1 4.6 %collective-permute-start.2 = (bf16[128,1024]{1,0:T(8,128)(2,1)S(1)}, bf16[128,1024]{1,0:T(8,128)(2,1)S(1)}, u32[]{:S(2)}, u32[]{:S(2)}) collective-permute-start(bf16[128,1024]{1,0:T(8,128)(2,1)S(1)} %maximum_select_fusion.b0), channel_id=1, source_target_pairs={{0,6},{1,25},{2,0},{3,27},{4,2},{5,29},{6,4},{7,31},{8,14},{9,1},{... | collective-permute-start | bytes 786440 | tf_op jit(solution)/shard_map/ppermute | solution.py:508
  19.7 1.9 %collective-permute-start.3 = (bf16[128,1024]{1,0:T(8,128)(2,1)S(1)}, bf16[128,1024]{1,0:T(8,128)(2,1)S(1)}, u32[]{:S(2)}, u32[]{:S(2)}) collective-permute-start(bf16[128,1024]{1,0:T(8,128)(2,1)S(1)} %maximum_select_fusion.b0), channel_id=1, source_target_pairs={{0,4},{1,17},{2,6},{3,19},{4,0},{5,21},{6,2},{7,23},{8,12},{9,25},... | collective-permute-start | bytes 786440 | tf_op jit(solution)/shard_map/ppermute | solution.py:509
  21.6 0.2 collective-permute-done.1.fm
  21.8 4.0 %collective-permute-done.2.fp = bf16[128,1024]{1,0:T(8,128)(2,1)S(1)} collective-permute-done((bf16[128,1024]{1,0:T(8,128)(2,1)S(1)}, bf16[128,1024]{1,0:T(8,128)(2,1)S(1)}, u32[]{:S(2)}, u32[]{:S(2)}) %collective-permute-start.2) | collective-permute-done | bytes 262176 | tf_op jit(solution)/shard_map/ppermute | solution.py:508
  25.8 2.8 %collective-permute-done.3.fo = bf16[128,1024]{1,0:T(8,128)(2,1)S(1)} collective-permute-done((bf16[128,1024]{1,0:T(8,128)(2,1)S(1)}, bf16[128,1024]{1,0:T(8,128)(2,1)S(1)}, u32[]{:S(2)}, u32[]{:S(2)}) %collective-permute-start.3) | collective-permute-done | bytes 262176 | tf_op jit(solution)/shard_map/ppermute | solution.py:509
  28.6 0.1 pad_maximum_fusion
  28.7 1.9 %collective-permute-start.4 = (bf16[512,1024]{1,0:T(8,128)(2,1)S(1)}, bf16[512,1024]{1,0:T(8,128)(2,1)S(1)}, u32[]{:S(2)}, u32[]{:S(2)}) collective-permute-start(bf16[512,1024]{1,0:T(8,128)(2,1)S(1)} %pad_maximum_fusion), channel_id=1, source_target_pairs={{0,8},{1,3},{2,10},{3,5},{4,12},{5,7},{6,14},{7,1},{8,16},{9,11},{... | collective-permute-start | bytes 3145736 | tf_op jit(solution)/shard_map/ppermute | solution.py:517
  30.6 4.6 %collective-permute-start.5 = (bf16[512,1024]{1,0:T(8,128)(2,1)S(1)}, bf16[512,1024]{1,0:T(8,128)(2,1)S(1)}, u32[]{:S(2)}, u32[]{:S(2)}) collective-permute-start(bf16[512,1024]{1,0:T(8,128)(2,1)S(1)} %pad_maximum_fusion), channel_id=1, source_target_pairs={{0,24},{1,7},{2,26},{3,1},{4,28},{5,3},{6,30},{7,5},{8,0},{9,15},{... | collective-permute-start | bytes 3145736 | tf_op jit(solution)/shard_map/ppermute | solution.py:518
  35.2 1.9 %collective-permute-start.8 = (bf16[128,2048]{1,0:T(8,128)(2,1)}, bf16[128,2048]{1,0:T(8,128)(2,1)}, u32[]{:S(2)}, u32[]{:S(2)}) collective-permute-start(bf16[128,2048]{1,0:T(8,128)(2,1)} %bitcast.t0), channel_id=1, source_target_pairs={{0,32},{32,0},{64,96},{96,64},{128,160},{160,128},{192,224},{224,1... | collective-permute-start | bytes 1572872 | tf_op jit(solution)/shard_map/ppermute | solution.py:510
  37.1 4.3 %collective-permute-start.9 = (bf16[128,2048]{1,0:T(8,128)(2,1)}, bf16[128,2048]{1,0:T(8,128)(2,1)}, u32[]{:S(2)}, u32[]{:S(2)}) collective-permute-start(bf16[128,2048]{1,0:T(8,128)(2,1)} %bitcast.t0), channel_id=1, source_target_pairs={{0,1},{1,0},{2,3},{3,2},{4,5},{5,4},{6,7},{7,6},{8,9},{9,8},{10,11... | collective-permute-start | bytes 1572872 | tf_op jit(solution)/shard_map/ppermute | solution.py:511
  41.4 7.0 %collective-permute-done.8.t1 = bf16[128,2048]{1,0:T(8,128)(2,1)} collective-permute-done((bf16[128,2048]{1,0:T(8,128)(2,1)}, bf16[128,2048]{1,0:T(8,128)(2,1)}, u32[]{:S(2)}, u32[]{:S(2)}) %collective-permute-start.8) | collective-permute-done | bytes 524320 | tf_op jit(solution)/shard_map/ppermute | solution.py:510
  48.5 5.2 %collective-permute-start.10 = (bf16[128,2048]{1,0:T(8,128)(2,1)}, bf16[128,2048]{1,0:T(8,128)(2,1)}, u32[]{:S(2)}, u32[]{:S(2)}) collective-permute-start(bf16[128,2048]{1,0:T(8,128)(2,1)} %collective-permute-done.8.t1), channel_id=1, source_target_pairs={{0,1},{1,0},{2,3},{3,2},{4,5},{5,4},{6,7},{7,6},{8,9},{9,8},{10,11... | collective-permute-start | bytes 1572872 | tf_op jit(solution)/shard_map/ppermute | solution.py:519
  53.7 1.9 %collective-permute-start.6 = (bf16[256,1024]{1,0:T(8,128)(2,1)S(1)}, bf16[256,1024]{1,0:T(8,128)(2,1)}, u32[]{:S(2)}, u32[]{:S(2)}) collective-permute-start(bf16[256,1024]{1,0:T(8,128)(2,1)S(1)} %slice.24), channel_id=1, source_target_pairs={{0,8},{1,3},{2,10},{3,5},{4,12},{5,7},{6,14},{7,1},{8,16},{9,11},{... | collective-permute-start | bytes 1572872 | tf_op jit(solution)/shard_map/ppermute | solution.py:520
  55.7 4.6 %collective-permute-start.7 = (bf16[256,1024]{1,0:T(8,128)(2,1)S(1)}, bf16[256,1024]{1,0:T(8,128)(2,1)}, u32[]{:S(2)}, u32[]{:S(2)}) collective-permute-start(bf16[256,1024]{1,0:T(8,128)(2,1)S(1)} %slice.25), channel_id=1, source_target_pairs={{0,24},{1,7},{2,26},{3,1},{4,28},{5,3},{6,30},{7,5},{8,0},{9,15},{... | collective-permute-start | bytes 1572872 | tf_op jit(solution)/shard_map/ppermute | solution.py:521
  60.3 0.1 pad.9.clone
  60.4 0.1 maximum_maximum_fusion
  60.5 0.1 reshape.13
  60.6 20.9 %all_to_all.15 = f32[16,1,512]{2,1,0:T(1,128)S(1)} all-to-all(f32[16,1,512]{2,1,0:T(1,128)S(1)} %reshape.13), channel_id=1, replica_groups=mesh['sp'=16,'dp'=32] {'sp'}, dimensions={0} | all-to-all | bytes 65536 | tf_op jit(solution)/shard_map/all_to_all | solution.py:516
  81.5 0.5 broadcast.5
  82.0 0.7 reduce
  82.8 0.7 reshape.14.par_ref
  83.5 6.3 %project.1 = (bf16[512,768]{1,0:T(8,128)(2,1)}, bf16[512,256]{1,0:T(8,128)(2,1)}) custom-call(bf16[128,1024]{1,0:T(8,128)(2,1)} %copy-done, bf16[128,1024]{1,0:T(8,128)(2,1)} %copy-done.3, bf16[128,1024]{1,0:T(8,128)(2,1)} %copy-done.4, bf16[128,1024]{1,0:T(8,128)(2,1)} %copy-done.5, bf16[512,1024]{1,0:T(8,128)(2,1)} %copy-done.1, ...), custom_call_target="tpu_custom_call" | custom-call | tf_op jit(solution)/shard_map/project/pallas_call | solution.py:458
  89.8 13.1 %maps.1 = (bf16[16,64,128]{2,1,0:T(8,128)(2,1)}, f32[4,2,2,2,128,128]{5,4,3,2,1,0:T(8,128)}, f32[4,2,128,128]{3,2,1,0:T(8,128)}) custom-call(bf16[512,768]{1,0:T(8,128)(2,1)} %get-tuple-element.13.k_ref.v_ref.q_ref, bf16[512,768]{1,0:T(8,128)(2,1)} %get-tuple-element.13.k_ref.v_ref.q_ref, bf16[512,256]{1,0:T(8,128)(2,1)} %get-tuple-element.14.low_ref, ...), custom_call_target="tpu_custom_call" | custom-call | flops 8000000000 | bytes 6000000 | tf_op jit(solution)/shard_map/maps/pallas_call | solution.py:282
  102.9 16.9 %all_to_all.16.u_ref = bf16[16,64,128]{2,1,0:T(8,128)(2,1)} all-to-all(bf16[16,64,128]{2,1,0:T(8,128)(2,1)} %get-tuple-element.19), channel_id=1, replica_groups=mesh['sp'=16,'dp'=32] {'sp'}, dimensions={0} | all-to-all | bytes 524288 | tf_op jit(solution)/shard_map/all_to_all | solution.py:525
  119.8 3.5 %states.1 = bf16[16,32,128]{2,1,0:T(8,128)(2,1)} custom-call(bf16[16,64,128]{2,1,0:T(8,128)(2,1)} %all_to_all.16.u_ref), custom_call_target="tpu_custom_call" | custom-call | tf_op jit(solution)/shard_map/states/pallas_call | solution.py:396
  123.3 10.3 %all-to-all-start.2 = ((bf16[16,32,128]{2,1,0:T(8,128)(2,1)}), bf16[16,32,128]{2,1,0:T(8,128)(2,1)S(1)}, u32[]{:S(2)}, u32[]{:S(2)}) async-start(bf16[16,32,128]{2,1,0:T(8,128)(2,1)} %states.1), calls=%async_computation.2 | async-start | bytes 262144 | tf_op jit(solution)/shard_map/all_to_all | solution.py:528
  133.6 11.6 %outputs.1 = (f32[2,512,256]{2,1,0:T(8,128)}, f32[2,512,256]{2,1,0:T(8,128)}, f32[512,256]{1,0:T(8,128)}) custom-call(bf16[512,768]{1,0:T(8,128)(2,1)} %get-tuple-element.13.k_ref.v_ref.q_ref, bf16[512,768]{1,0:T(8,128)(2,1)} %get-tuple-element.13.k_ref.v_ref.q_ref, bf16[512,768]{1,0:T(8,128)(2,1)} %get-tuple-element.13.k_ref.v_ref.q_ref, ...), custom_call_target="tpu_custom_call" | custom-call | flops 4000000000 | bytes 8000000 | tf_op jit(solution)/shard_map/outputs/pallas_call | solution.py:309
  145.2 0.4 all-to-all-done.2.s_ref
  145.6 0.7 copy-done.6
  146.2 4.3 %final.1 = bf16[512,256]{1,0:T(8,128)(2,1)} custom-call(f32[2,512,256]{2,1,0:T(8,128)} %get-tuple-element.17.y_ref, f32[2,512,256]{2,1,0:T(8,128)} %get-tuple-element.18.qx_ref, bf16[16,32,128]{2,1,0:T(8,128)(2,1)} %copy-done.6, f32[512,256]{1,0:T(8,128)} %get-tuple-element.20.own_ref, f32[16,8,64]{2,1,0:T(8,128)} %reshape.14.par_ref), custom_call_target="tpu_custom_call" | custom-call | tf_op jit(solution)/shard_map/final/pallas_call | solution.py:358
  150.5 0.9 dynamic-slice_bitcast_fusion
  151.4 2.9 %collective-permute-start.11 = (bf16[2,128,256]{2,1,0:T(8,128)(2,1)S(1)}, bf16[2,128,256]{2,1,0:T(8,128)(2,1)S(1)}, u32[]{:S(2)}, u32[]{:S(2)}) collective-permute-start(bf16[2,128,256]{2,1,0:T(8,128)(2,1)S(1)} %dynamic-slice_bitcast_fusion), channel_id=1, source_target_pairs={{0,32},{32,0},{64,96},{96,64},{128,160},{160,128},{192,224},{224,1... | collective-permute-start | bytes 393224 | tf_op jit(solution)/shard_map/ppermute | solution.py:533
  154.4 2.7 %collective-permute-done.11 = bf16[2,128,256]{2,1,0:T(8,128)(2,1)S(1)} collective-permute-done((bf16[2,128,256]{2,1,0:T(8,128)(2,1)S(1)}, bf16[2,128,256]{2,1,0:T(8,128)(2,1)S(1)}, u32[]{:S(2)}, u32[]{:S(2)}) %collective-permute-start.11) | collective-permute-done | bytes 131104 | tf_op jit(solution)/shard_map/ppermute | solution.py:533
  157.1 0.9 bitcast_select_fusion
  158.1 7.1 %collective-permute-start.12 = (bf16[128,512]{1,0:T(8,128)(2,1)S(1)}, bf16[128,512]{1,0:T(8,128)(2,1)S(1)}, u32[]{:S(2)}, u32[]{:S(2)}) collective-permute-start(bf16[128,512]{1,0:T(8,128)(2,1)S(1)} %fusion.1), channel_id=1, source_target_pairs={{0,1},{1,0},{2,3},{3,2},{4,5},{5,4},{6,7},{7,6},{8,9},{9,8},{10,11... | collective-permute-start | bytes 393224 | tf_op jit(solution)/shard_map/ppermute | solution.py:538
  165.2 1.0 collective-permute-done.12
  166.2 0.1 broadcast_select_fusion.1
  166.3 0.7 maximum_bitcast_fusion
  (29 shorter events, 0.2 us)
Async XLA Ops:
  2.4 9.7 %collective-permute-start = (bf16[64,1024]{1,0:T(8,128)(2,1)S(1)}, bf16[64,1024]{1,0:T(8,128)(2,1)S(1)}, u32[]{:S(2)}, u32[]{:S(2)}) collective-permute-start(bf16[64,1024]{1,0:T(8,128)(2,1)S(1)} %pad_maximum_fusion.1), channel_id=1, source_target_pairs={{0,1},{1,0},{2,3},{3,2},{4,5},{5,4},{6,7},{7,6},{8,9},{9,8},{10,11... | collective-permute-start | bytes 393224 | tf_op jit(solution)/shard_map/ppermute | solution.py:504
  13.0 42.7 %copy-start = (bf16[128,1024]{1,0:T(8,128)(2,1)}, bf16[128,1024]{1,0:T(8,128)(2,1)S(1)}, u32[]{:S(2)}) copy-start(bf16[128,1024]{1,0:T(8,128)(2,1)S(1)} %maximum_select_fusion.b0) | copy-start | bytes 786436
  13.0 47.4 %copy-start.7 = (f32[2,64]{1,0:T(2,128)S(1)}, f32[2,64]{1,0:T(2,128)}, u32[]{:S(2)}) copy-start(f32[2,64]{1,0:T(2,128)} %param.18) | copy-start | bytes 1540
  13.0 47.4 %copy-start.8 = (f32[2,64]{1,0:T(2,128)S(1)}, f32[2,64]{1,0:T(2,128)}, u32[]{:S(2)}) copy-start(f32[2,64]{1,0:T(2,128)} %param.17) | copy-start | bytes 1540
  13.0 47.4 %copy-start.9 = (f32[64]{0:T(128)S(1)}, f32[64]{0:T(128)}, u32[]{:S(2)}) copy-start(f32[64]{0:T(128)} %param.19) | copy-start | bytes 772
  13.0 8.8 %collective-permute-start.1 = (bf16[128,1024]{1,0:T(8,128)(2,1)S(1)}, bf16[128,1024]{1,0:T(8,128)(2,1)S(1)}, u32[]{:S(2)}, u32[]{:S(2)}) collective-permute-start(bf16[128,1024]{1,0:T(8,128)(2,1)S(1)} %maximum_select_fusion.b0), channel_id=1, source_target_pairs={{0,2},{1,9},{2,4},{3,11},{4,6},{5,13},{6,0},{7,15},{8,10},{9,17},{... | collective-permute-start | bytes 786440 | tf_op jit(solution)/shard_map/ppermute | solution.py:507
  15.1 10.7 %collective-permute-start.2 = (bf16[128,1024]{1,0:T(8,128)(2,1)S(1)}, bf16[128,1024]{1,0:T(8,128)(2,1)S(1)}, u32[]{:S(2)}, u32[]{:S(2)}) collective-permute-start(bf16[128,1024]{1,0:T(8,128)(2,1)S(1)} %maximum_select_fusion.b0), channel_id=1, source_target_pairs={{0,6},{1,25},{2,0},{3,27},{4,2},{5,29},{6,4},{7,31},{8,14},{9,1},{... | collective-permute-start | bytes 786440 | tf_op jit(solution)/shard_map/ppermute | solution.py:508
  19.7 8.9 %collective-permute-start.3 = (bf16[128,1024]{1,0:T(8,128)(2,1)S(1)}, bf16[128,1024]{1,0:T(8,128)(2,1)S(1)}, u32[]{:S(2)}, u32[]{:S(2)}) collective-permute-start(bf16[128,1024]{1,0:T(8,128)(2,1)S(1)} %maximum_select_fusion.b0), channel_id=1, source_target_pairs={{0,4},{1,17},{2,6},{3,19},{4,0},{5,21},{6,2},{7,23},{8,12},{9,25},... | collective-permute-start | bytes 786440 | tf_op jit(solution)/shard_map/ppermute | solution.py:509
  21.8 33.9 %copy-start.3 = (bf16[128,1024]{1,0:T(8,128)(2,1)}, bf16[128,1024]{1,0:T(8,128)(2,1)S(1)}, u32[]{:S(2)}) copy-start(bf16[128,1024]{1,0:T(8,128)(2,1)S(1)} %collective-permute-done.1.fm) | copy-start | bytes 786436
  25.8 29.9 %copy-start.4 = (bf16[128,1024]{1,0:T(8,128)(2,1)}, bf16[128,1024]{1,0:T(8,128)(2,1)S(1)}, u32[]{:S(2)}) copy-start(bf16[128,1024]{1,0:T(8,128)(2,1)S(1)} %collective-permute-done.2.fp) | copy-start | bytes 786436
  28.6 27.1 %copy-start.5 = (bf16[128,1024]{1,0:T(8,128)(2,1)}, bf16[128,1024]{1,0:T(8,128)(2,1)S(1)}, u32[]{:S(2)}) copy-start(bf16[128,1024]{1,0:T(8,128)(2,1)S(1)} %collective-permute-done.3.fo) | copy-start | bytes 786436
  28.7 25.0 %collective-permute-start.4 = (bf16[512,1024]{1,0:T(8,128)(2,1)S(1)}, bf16[512,1024]{1,0:T(8,128)(2,1)S(1)}, u32[]{:S(2)}, u32[]{:S(2)}) collective-permute-start(bf16[512,1024]{1,0:T(8,128)(2,1)S(1)} %pad_maximum_fusion), channel_id=1, source_target_pairs={{0,8},{1,3},{2,10},{3,5},{4,12},{5,7},{6,14},{7,1},{8,16},{9,11},{... | collective-permute-start | bytes 3145736 | tf_op jit(solution)/shard_map/ppermute | solution.py:517
  30.6 25.0 %collective-permute-start.5 = (bf16[512,1024]{1,0:T(8,128)(2,1)S(1)}, bf16[512,1024]{1,0:T(8,128)(2,1)S(1)}, u32[]{:S(2)}, u32[]{:S(2)}) collective-permute-start(bf16[512,1024]{1,0:T(8,128)(2,1)S(1)} %pad_maximum_fusion), channel_id=1, source_target_pairs={{0,24},{1,7},{2,26},{3,1},{4,28},{5,3},{6,30},{7,5},{8,0},{9,15},{... | collective-permute-start | bytes 3145736 | tf_op jit(solution)/shard_map/ppermute | solution.py:518
  35.2 13.3 %collective-permute-start.8 = (bf16[128,2048]{1,0:T(8,128)(2,1)}, bf16[128,2048]{1,0:T(8,128)(2,1)}, u32[]{:S(2)}, u32[]{:S(2)}) collective-permute-start(bf16[128,2048]{1,0:T(8,128)(2,1)} %bitcast.t0), channel_id=1, source_target_pairs={{0,32},{32,0},{64,96},{96,64},{128,160},{160,128},{192,224},{224,1... | collective-permute-start | bytes 1572872 | tf_op jit(solution)/shard_map/ppermute | solution.py:510
  37.1 46.3 %collective-permute-start.9 = (bf16[128,2048]{1,0:T(8,128)(2,1)}, bf16[128,2048]{1,0:T(8,128)(2,1)}, u32[]{:S(2)}, u32[]{:S(2)}) collective-permute-start(bf16[128,2048]{1,0:T(8,128)(2,1)} %bitcast.t0), channel_id=1, source_target_pairs={{0,1},{1,0},{2,3},{3,2},{4,5},{5,4},{6,7},{7,6},{8,9},{9,8},{10,11... | collective-permute-start | bytes 1572872 | tf_op jit(solution)/shard_map/ppermute | solution.py:511
  48.5 35.0 %collective-permute-start.10 = (bf16[128,2048]{1,0:T(8,128)(2,1)}, bf16[128,2048]{1,0:T(8,128)(2,1)}, u32[]{:S(2)}, u32[]{:S(2)}) collective-permute-start(bf16[128,2048]{1,0:T(8,128)(2,1)} %collective-permute-done.8.t1), channel_id=1, source_target_pairs={{0,1},{1,0},{2,3},{3,2},{4,5},{5,4},{6,7},{7,6},{8,9},{9,8},{10,11... | collective-permute-start | bytes 1572872 | tf_op jit(solution)/shard_map/ppermute | solution.py:519
  53.6 29.8 %copy-start.1 = (bf16[512,1024]{1,0:T(8,128)(2,1)}, bf16[512,1024]{1,0:T(8,128)(2,1)S(1)}, u32[]{:S(2)}) copy-start(bf16[512,1024]{1,0:T(8,128)(2,1)S(1)} %collective-permute-done.4.r1) | copy-start | bytes 3145732
  53.7 29.8 %collective-permute-start.6 = (bf16[256,1024]{1,0:T(8,128)(2,1)S(1)}, bf16[256,1024]{1,0:T(8,128)(2,1)}, u32[]{:S(2)}, u32[]{:S(2)}) collective-permute-start(bf16[256,1024]{1,0:T(8,128)(2,1)S(1)} %slice.24), channel_id=1, source_target_pairs={{0,8},{1,3},{2,10},{3,5},{4,12},{5,7},{6,14},{7,1},{8,16},{9,11},{... | collective-permute-start | bytes 1572872 | tf_op jit(solution)/shard_map/ppermute | solution.py:520
  55.6 27.8 %copy-start.2 = (bf16[512,1024]{1,0:T(8,128)(2,1)}, bf16[512,1024]{1,0:T(8,128)(2,1)S(1)}, u32[]{:S(2)}) copy-start(bf16[512,1024]{1,0:T(8,128)(2,1)S(1)} %collective-permute-done.5.r2) | copy-start | bytes 3145732
  55.7 27.7 %collective-permute-start.7 = (bf16[256,1024]{1,0:T(8,128)(2,1)S(1)}, bf16[256,1024]{1,0:T(8,128)(2,1)}, u32[]{:S(2)}, u32[]{:S(2)}) collective-permute-start(bf16[256,1024]{1,0:T(8,128)(2,1)S(1)} %slice.25), channel_id=1, source_target_pairs={{0,24},{1,7},{2,26},{3,1},{4,28},{5,3},{6,30},{7,5},{8,0},{9,15},{... | collective-permute-start | bytes 1572872 | tf_op jit(solution)/shard_map/ppermute | solution.py:521
  123.3 22.3 %all-to-all-start.2 = ((bf16[16,32,128]{2,1,0:T(8,128)(2,1)}), bf16[16,32,128]{2,1,0:T(8,128)(2,1)S(1)}, u32[]{:S(2)}, u32[]{:S(2)}) async-start(bf16[16,32,128]{2,1,0:T(8,128)(2,1)} %states.1), calls=%async_computation.2 | async-start | bytes 262144 | tf_op jit(solution)/shard_map/all_to_all | solution.py:528
  145.6 0.7 copy-start.6
  151.4 5.7 %collective-permute-start.11 = (bf16[2,128,256]{2,1,0:T(8,128)(2,1)S(1)}, bf16[2,128,256]{2,1,0:T(8,128)(2,1)S(1)}, u32[]{:S(2)}, u32[]{:S(2)}) collective-permute-start(bf16[2,128,256]{2,1,0:T(8,128)(2,1)S(1)} %dynamic-slice_bitcast_fusion), channel_id=1, source_target_pairs={{0,32},{32,0},{64,96},{96,64},{128,160},{160,128},{192,224},{224,1... | collective-permute-start | bytes 393224 | tf_op jit(solution)/shard_map/ppermute | solution.py:533
  158.1 8.1 %collective-permute-start.12 = (bf16[128,512]{1,0:T(8,128)(2,1)S(1)}, bf16[128,512]{1,0:T(8,128)(2,1)S(1)}, u32[]{:S(2)}, u32[]{:S(2)}) collective-permute-start(bf16[128,512]{1,0:T(8,128)(2,1)S(1)} %fusion.1), channel_id=1, source_target_pairs={{0,1},{1,0},{2,3},{3,2},{4,5},{5,4},{6,7},{7,6},{8,9},{9,8},{10,11... | collective-permute-start | bytes 393224 | tf_op jit(solution)/shard_map/ppermute | solution.py:538

commit v3 on v2

--- a/solution.py
+++ b/solution.py
@@ -324,14 +324,16 @@
     )(qkv, qkv, qkv, low, up, floor, par, x, u)
 
 
-def final_kernel(role, y_ref, qx_ref, s_ref, own_ref, par_ref, o_ref):
+def final_kernel(place, y_ref, qx_ref, s_ref, own_ref, par_ref, here, along, across, both, o_ref):
     mean = head_ones(1.0 / H)
     z = jnp.zeros((H, H), BF)
     hps = own_ref.shape[1] // 128
+    p, c, _, _ = place()
+    seq = pl.program_id(0)
     for hp in range(hps):
         ln = slice(hp * 128, (hp + 1) * 128)
         total = own_ref[:, ln]
-        gain = head_row(par_ref, role() * hps + hp, 4)
+        gain = head_row(par_ref, (2 * p + c) * hps + hp, 4)
         for d in range(2):
             sa, sb = s_ref[4 * hp + d], s_ref[4 * hp + 2 + d]
             blk = jnp.concatenate(
@@ -347,16 +349,23 @@
             cen = y - head_sum(y, mean)
             var = head_sum(cen * cen, mean)
             total = total + cen * lax.rsqrt(var + 0.00064) * gain
-        o_ref[:, ln] = total.astype(BF)
-
-
-def final(role, y, qx, s, own, par, tokens):
+        o_ref[seq, :, :, ln] = total.astype(BF).reshape(2, -1, 128)
+
+    @pl.when(seq == 1)
+    def _():
+        here[...] = o_ref[c, p]
+        along[...] = o_ref[c, 1 - p]
+        across[...] = o_ref[1 - c, p]
+        both[...] = o_ref[1 - c, 1 - p]
+
+
+def final(place, y, qx, s, own, par, tokens):
     rows, width = own.shape
     hps = width // 128
     dspec = pl.BlockSpec((2, tokens, width), lambda s: (0, s, 0))
     one = pl.BlockSpec((tokens, width), lambda s: (s, 0))
     return pl.pallas_call(
-        functools.partial(final_kernel, role),
+        functools.partial(final_kernel, place),
         grid=(rows // tokens,),
         in_specs=[
             dspec,
@@ -365,8 +374,9 @@
             one,
             *whole(par),
         ],
-        out_specs=one,
-        out_shape=jax.ShapeDtypeStruct((rows, width), BF),
+        out_specs=[pl.BlockSpec((tokens // 2, width), lambda s: (0, 0))] * 4,
+        out_shape=[jax.ShapeDtypeStruct((tokens // 2, width), BF)] * 4,
+        scratch_shapes=[pltpu.VMEM((2, 2, tokens // 2, width), BF)],
         compiler_params=BIG,
         name="final",
     )(y, qx, s, own, par)
@@ -417,7 +427,7 @@
     return lax.axis_index("sp") % 2
 
 
-def project_kernel(b0, fm, fp, fo, r1, r2, r3t, r3b, t0, t1, t2, t3, qkv_ref, low_ref, w_ref, t_ref, sem):
+def project_kernel(b0, fm, fp, fo, r1, r2, ro, t0, t1, t2, t3, qkv_ref, low_ref, w_ref, t_ref, sem):
     p, c, y, x = place()
     rows = b0.shape[0]
     n = t0.shape[0]
@@ -437,7 +447,7 @@
         (0, [(b0, 0), (fm, 0), (fp, 0), (fo, 0)]),
         (-1, [(r1, i) for i in range(4)]),
         (1, [(r2, i) for i in range(4)]),
-        (2, [(r3t, 0), (r3t, 1), (r3b, 0), (r3b, 1)]),
+        (2, [(ro, i) for i in range(4)]),
     ):
         for delta, (ref, i) in zip((0, -1, 1, 2), parts):
             aa, bb = lax.rem(a + delta + 4, 4), lax.rem(b + eps + 4, 4)
@@ -457,7 +467,7 @@
     vm = pl.BlockSpec(memory_space=pltpu.VMEM)
     return pl.pallas_call(
         project_kernel,
-        in_specs=[pl.BlockSpec(memory_space=pl.ANY)] * 12,
+        in_specs=[pl.BlockSpec(memory_space=pl.ANY)] * 11,
         out_specs=[vm, vm],
         out_shape=[
             jax.ShapeDtypeStruct((4 * n, width3), BF),
@@ -503,7 +513,6 @@
     keep = columns(2 * p + c)
     recv = lax.ppermute(columns(2 * p + 1 - c), "dp", CORES)
     b0 = jnp.where(c == 0, jnp.concatenate([keep, recv], 0), jnp.concatenate([recv, keep], 0))
-    rows = b0.shape[0]
     fm = lax.ppermute(b0, "dp", shift(True, 1))
     fp = lax.ppermute(b0, "dp", shift(True, -1))
     fo = lax.ppermute(b0, "dp", shift(True, 2))
@@ -516,32 +525,27 @@
     par = lax.all_to_all(par, "sp", split_axis=0, concat_axis=0, tiled=True)
     r1 = lax.ppermute(s4, "dp", shift(False, 1))
     r2 = lax.ppermute(s4, "dp", shift(False, -1))
+    ro = lax.ppermute(s4, "dp", shift(False, 2))
     tcz = lax.ppermute(tz, "dp", CORES)
-    r3t = lax.ppermute(r1[: 2 * rows], "dp", shift(False, 1))
-    r3b = lax.ppermute(r2[2 * rows :], "dp", shift(False, -1))
-    qkv, low = project((b0, fm, fp, fo, r1, r2, r3t, r3b), (tok, tz, tc, tcz), 3 * width)
+    qkv, low = project((b0, fm, fp, fo, r1, r2, ro), (tok, tz, tc, tcz), 3 * width)
     span = 2 * n
     msg, xs, us = maps(role, qkv, low, up, floor, par, span)
     got = lax.all_to_all(msg, "sp", split_axis=0, concat_axis=0, tiled=True)
     y0, qx, own = outputs(role, qkv, low, up, floor, par, xs, us, span)
     st = scan_states(got, backwards, 2)
     st = lax.all_to_all(st, "sp", split_axis=0, concat_axis=0, tiled=True)
-    out = final(role, y0, qx, st, own, par, span)
-
-    out = out.reshape(2, 2, n, width)
-    mine = lax.dynamic_index_in_dim(out, p, 1, False)
-    rz = lax.ppermute(lax.dynamic_index_in_dim(out, 1 - p, 1, False), "sp", ZPAIRS)
-    pick = lambda m, s: lax.dynamic_index_in_dim(m, s, 0, False)
-    low_p = jnp.where(p == 0, mine, rz)
-    high_p = jnp.where(p == 0, rz, mine)
-    both = jnp.concatenate([low_p, high_p], 2)
-    far = lax.ppermute(pick(both, 1 - c), "dp", CORES)
-    near = pick(both, c)
-    first = jnp.where(c == 0, near, far)
-    second = jnp.where(c == 0, far, near)
-    res = jnp.concatenate(
-        [first[:, :width], second[:, :width], first[:, width:], second[:, width:]], 1
-    )
+    here, along, across, both = final(place, y0, qx, st, own, par, span)
+    both = lax.ppermute(
+        both, ("sp", "dp"), [(32 * i + k, 32 * (i ^ 1) + (k ^ 1)) for i in range(16) for k in range(32)]
+    )
+    along = lax.ppermute(along, "sp", ZPAIRS)
+    across = lax.ppermute(across, "dp", CORES)
+    low = [jnp.where(p == 0, here, along), jnp.where(p == 0, across, both)]
+    high = [jnp.where(p == 0, along, here), jnp.where(p == 0, both, across)]
+    parts = []
+    for m, o in (low, high):
+        parts += [jnp.where(c == 0, m, o), jnp.where(c == 0, o, m)]
+    res = jnp.concatenate(parts, 1)
     return res.reshape(1, n, 4 * width)
 
 

time: 168 us -> 154 us (0.917)
  waiting for transfers between devices: 19 us -> 9.33 us
  starting transfers between devices: 62 us -> 55.5 us
  blocking collectives: 37.9 us -> 39.7 us
    ppermute x1, waiting for transfers between devices: 7.02 us -> 0.01 us  [body(): tz = lax.ppermute(tok, 'sp', ZPAIRS)]
    ppermute x1, starting transfers between devices: 5.17 us -> 1.92 us  [body(): tcz = lax.ppermute(tz, 'dp', CORES)]
    ppermute x4, starting transfers between devices: 16.5 us -> 13.3 us  [the longest x1 5.59 us: body(): across = lax.ppermute(across, 'dp', CORES)]
    all_to_all x1, blocking collectives: 20.9 us -> 22.7 us  [body(): par = lax.all_to_all(par, 'sp', split_axis=0, concat_axis=0, tiled=True)]
    ppermute x1, waiting for transfers between devices: 3.99 us -> 2.22 us  [body(): fp = lax.ppermute(b0, 'dp', shift(True, -1))]
  transfers between devices with their start and end apart: 14 -> 14, of which waited for: 8 -> 5; matrix products, arithmetic and copies ran while one was open for 1% -> 2% of each run, Pallas kernels for 7% -> 8%
where the time goes in v3:
time: 154 us; the launch traced here: 153 us
  starting transfers between devices  55.5 us (36%)
  blocking collectives  39.7 us (26%)
  Pallas kernels  38.7 us (25%)
  waiting for transfers between devices  9.33 us (6%)
  local copies, waits for them, and re-layouts  5.01 us (3%)
  other arithmetic  4.16 us (3%)
    all_to_all x1, blocking collectives, body(): par = lax.all_to_all(par, 'sp', split_axis=0, concat_axis=0, tiled=True)  22.7 us
    all_to_all x1, blocking collectives, body(): got = lax.all_to_all(msg, 'sp', split_axis=0, concat_axis=0, tiled=True)  16.9 us
    pallas_call x1, Pallas kernels, maps(): pl.pallas_call(functools.partial(maps_kernel, role), grid=(seqs,), in_spe...  13.1 us
    pallas_call x1, Pallas kernels, outputs(): pl.pallas_call(functools.partial(outputs_kernel, role), grid=(seqs, hps),...  11.6 us
    all_to_all x1, starting transfers between devices, body(): st = lax.all_to_all(st, 'sp', split_axis=0, concat_axis=0, tiled=True)  10.4 us
    ppermute x1, starting transfers between devices, body(): recv = lax.ppermute(columns(2 * p + 1 - c), 'dp', CORES)  8.75 us
    pallas_call x1, Pallas kernels, project(): pl.pallas_call(project_kernel, in_specs=[pl.BlockSpec(memory_space=pl.ANY...  6.25 us
    ppermute x1, starting transfers between devices, body(): across = lax.ppermute(across, 'dp', CORES)  5.59 us
  transfers between devices with their start and end apart: 14, of which 5 were waited for; matrix products, arithmetic and copies ran while one was open for 2% of the time, Pallas kernels for 8%

profile of v3, /device:TPU:1, one launch (start us, length us, event | category | flops | bytes accessed | tf_op | source)
XLA Modules:
  0.0 152.8 jit_solution(541172469099929585)
XLA Ops:
  0.0 0.8 constant_dynamic-slice_fusion.5
  0.8 0.8 constant_dynamic-slice_fusion.3
  1.6 0.8 pad_maximum_fusion.1
  2.4 8.7 %collective-permute-start = (bf16[64,1024]{1,0:T(8,128)(2,1)S(1)}, bf16[64,1024]{1,0:T(8,128)(2,1)S(1)}, u32[]{:S(2)}, u32[]{:S(2)}) collective-permute-start(bf16[64,1024]{1,0:T(8,128)(2,1)S(1)} %pad_maximum_fusion.1), channel_id=1, source_target_pairs={{0,1},{1,0},{2,3},{3,2},{4,5},{5,4},{6,7},{7,6},{8,9},{9,8},{10,11... | collective-permute-start | bytes 393224 | tf_op jit(solution)/shard_map/ppermute | solution.py:514
  11.2 1.0 collective-permute-done
  12.1 0.9 maximum_select_fusion.b0
  13.0 0.0 copy-start
  13.0 1.9 %collective-permute-start.1 = (bf16[128,1024]{1,0:T(8,128)(2,1)S(1)}, bf16[128,1024]{1,0:T(8,128)(2,1)S(1)}, u32[]{:S(2)}, u32[]{:S(2)}) collective-permute-start(bf16[128,1024]{1,0:T(8,128)(2,1)S(1)} %maximum_select_fusion.b0), channel_id=1, source_target_pairs={{0,2},{1,9},{2,4},{3,11},{4,6},{5,13},{6,0},{7,15},{8,10},{9,17},{... | collective-permute-start | bytes 786440 | tf_op jit(solution)/shard_map/ppermute | solution.py:516
  15.0 4.6 %collective-permute-start.2 = (bf16[128,1024]{1,0:T(8,128)(2,1)S(1)}, bf16[128,1024]{1,0:T(8,128)(2,1)S(1)}, u32[]{:S(2)}, u32[]{:S(2)}) collective-permute-start(bf16[128,1024]{1,0:T(8,128)(2,1)S(1)} %maximum_select_fusion.b0), channel_id=1, source_target_pairs={{0,6},{1,25},{2,0},{3,27},{4,2},{5,29},{6,4},{7,31},{8,14},{9,1},{... | collective-permute-start | bytes 786440 | tf_op jit(solution)/shard_map/ppermute | solution.py:517
  19.6 1.9 %collective-permute-start.3 = (bf16[128,1024]{1,0:T(8,128)(2,1)S(1)}, bf16[128,1024]{1,0:T(8,128)(2,1)S(1)}, u32[]{:S(2)}, u32[]{:S(2)}) collective-permute-start(bf16[128,1024]{1,0:T(8,128)(2,1)S(1)} %maximum_select_fusion.b0), channel_id=1, source_target_pairs={{0,4},{1,17},{2,6},{3,19},{4,0},{5,21},{6,2},{7,23},{8,12},{9,25},... | collective-permute-start | bytes 786440 | tf_op jit(solution)/shard_map/ppermute | solution.py:518
  21.5 1.9 %collective-permute-start.7 = (bf16[128,2048]{1,0:T(8,128)(2,1)}, bf16[128,2048]{1,0:T(8,128)(2,1)}, u32[]{:S(2)}, u32[]{:S(2)}) collective-permute-start(bf16[128,2048]{1,0:T(8,128)(2,1)} %bitcast.t0), channel_id=1, source_target_pairs={{0,32},{32,0},{64,96},{96,64},{128,160},{160,128},{192,224},{224,1... | collective-permute-start | bytes 1572872 | tf_op jit(solution)/shard_map/ppermute | solution.py:519
  23.4 0.0 collective-permute-done.1.fm
  23.4 2.2 %collective-permute-done.2.fp = bf16[128,1024]{1,0:T(8,128)(2,1)S(1)} collective-permute-done((bf16[128,1024]{1,0:T(8,128)(2,1)S(1)}, bf16[128,1024]{1,0:T(8,128)(2,1)S(1)}, u32[]{:S(2)}, u32[]{:S(2)}) %collective-permute-start.2) | collective-permute-done | bytes 262176 | tf_op jit(solution)/shard_map/ppermute | solution.py:517
  25.7 2.8 %collective-permute-done.3.fo = bf16[128,1024]{1,0:T(8,128)(2,1)S(1)} collective-permute-done((bf16[128,1024]{1,0:T(8,128)(2,1)S(1)}, bf16[128,1024]{1,0:T(8,128)(2,1)S(1)}, u32[]{:S(2)}, u32[]{:S(2)}) %collective-permute-start.3) | collective-permute-done | bytes 262176 | tf_op jit(solution)/shard_map/ppermute | solution.py:518
  28.5 0.1 pad_maximum_fusion
  28.5 1.9 %collective-permute-start.4 = (bf16[512,1024]{1,0:T(8,128)(2,1)S(1)}, bf16[512,1024]{1,0:T(8,128)(2,1)S(1)}, u32[]{:S(2)}, u32[]{:S(2)}) collective-permute-start(bf16[512,1024]{1,0:T(8,128)(2,1)S(1)} %pad_maximum_fusion), channel_id=1, source_target_pairs={{0,8},{1,3},{2,10},{3,5},{4,12},{5,7},{6,14},{7,1},{8,16},{9,11},{... | collective-permute-start | bytes 3145736 | tf_op jit(solution)/shard_map/ppermute | solution.py:526
  30.5 4.6 %collective-permute-start.5 = (bf16[512,1024]{1,0:T(8,128)(2,1)S(1)}, bf16[512,1024]{1,0:T(8,128)(2,1)S(1)}, u32[]{:S(2)}, u32[]{:S(2)}) collective-permute-start(bf16[512,1024]{1,0:T(8,128)(2,1)S(1)} %pad_maximum_fusion), channel_id=1, source_target_pairs={{0,24},{1,7},{2,26},{3,1},{4,28},{5,3},{6,30},{7,5},{8,0},{9,15},{... | collective-permute-start | bytes 3145736 | tf_op jit(solution)/shard_map/ppermute | solution.py:527
  35.1 1.9 %collective-permute-start.6 = (bf16[512,1024]{1,0:T(8,128)(2,1)S(1)}, bf16[512,1024]{1,0:T(8,128)(2,1)}, u32[]{:S(2)}, u32[]{:S(2)}) collective-permute-start(bf16[512,1024]{1,0:T(8,128)(2,1)S(1)} %pad_maximum_fusion), channel_id=1, source_target_pairs={{0,16},{1,5},{2,18},{3,7},{4,20},{5,1},{6,22},{7,3},{8,24},{9,13},... | collective-permute-start | bytes 3145736 | tf_op jit(solution)/shard_map/ppermute | solution.py:528
  37.0 4.3 %collective-permute-start.8 = (bf16[128,2048]{1,0:T(8,128)(2,1)}, bf16[128,2048]{1,0:T(8,128)(2,1)}, u32[]{:S(2)}, u32[]{:S(2)}) collective-permute-start(bf16[128,2048]{1,0:T(8,128)(2,1)} %bitcast.t0), channel_id=1, source_target_pairs={{0,1},{1,0},{2,3},{3,2},{4,5},{5,4},{6,7},{7,6},{8,9},{9,8},{10,11... | collective-permute-start | bytes 1572872 | tf_op jit(solution)/shard_map/ppermute | solution.py:520
  41.3 0.0 collective-permute-done.7.t1
  41.4 1.9 %collective-permute-start.9 = (bf16[128,2048]{1,0:T(8,128)(2,1)}, bf16[128,2048]{1,0:T(8,128)(2,1)}, u32[]{:S(2)}, u32[]{:S(2)}) collective-permute-start(bf16[128,2048]{1,0:T(8,128)(2,1)} %collective-permute-done.7.t1), channel_id=1, source_target_pairs={{0,1},{1,0},{2,3},{3,2},{4,5},{5,4},{6,7},{7,6},{8,9},{9,8},{10,11... | collective-permute-start | bytes 1572872 | tf_op jit(solution)/shard_map/ppermute | solution.py:529
  43.3 0.1 pad.7.clone
  43.4 0.1 maximum_maximum_fusion
  43.5 0.1 reshape.9
  43.6 22.7 %all_to_all.15 = f32[16,1,512]{2,1,0:T(1,128)S(1)} all-to-all(f32[16,1,512]{2,1,0:T(1,128)S(1)} %reshape.9), channel_id=1, replica_groups=mesh['sp'=16,'dp'=32] {'sp'}, dimensions={0} | all-to-all | bytes 65536 | tf_op jit(solution)/shard_map/all_to_all | solution.py:525
  66.3 0.6 broadcast.5
  66.9 0.8 reduce
  67.7 0.7 reshape.10.par_ref
  68.4 0.0 collective-permute-done.5.r2
  68.4 0.0 collective-permute-done.6.ro
  68.4 0.9 copy-done.1
  69.3 0.3 copy-done.2
  69.7 6.3 %project.1 = (bf16[512,768]{1,0:T(8,128)(2,1)}, bf16[512,256]{1,0:T(8,128)(2,1)}) custom-call(bf16[128,1024]{1,0:T(8,128)(2,1)} %copy-done, bf16[128,1024]{1,0:T(8,128)(2,1)} %copy-done.3, bf16[128,1024]{1,0:T(8,128)(2,1)} %copy-done.4, bf16[128,1024]{1,0:T(8,128)(2,1)} %copy-done.5, bf16[512,1024]{1,0:T(8,128)(2,1)} %copy-done.1, ...), custom_call_target="tpu_custom_call" | custom-call | tf_op jit(solution)/shard_map/project/pallas_call | solution.py:468
  75.9 13.1 %maps.1 = (bf16[16,64,128]{2,1,0:T(8,128)(2,1)}, f32[4,2,2,2,128,128]{5,4,3,2,1,0:T(8,128)}, f32[4,2,128,128]{3,2,1,0:T(8,128)}) custom-call(bf16[512,768]{1,0:T(8,128)(2,1)} %get-tuple-element.17.k_ref.v_ref.q_ref, bf16[512,768]{1,0:T(8,128)(2,1)} %get-tuple-element.17.k_ref.v_ref.q_ref, bf16[512,256]{1,0:T(8,128)(2,1)} %get-tuple-element.18.low_ref, ...), custom_call_target="tpu_custom_call" | custom-call | flops 8000000000 | bytes 6000000 | tf_op jit(solution)/shard_map/maps/pallas_call | solution.py:282
  89.0 16.9 %all_to_all.16.u_ref = bf16[16,64,128]{2,1,0:T(8,128)(2,1)} all-to-all(bf16[16,64,128]{2,1,0:T(8,128)(2,1)} %get-tuple-element.23), channel_id=1, replica_groups=mesh['sp'=16,'dp'=32] {'sp'}, dimensions={0} | all-to-all | bytes 524288 | tf_op jit(solution)/shard_map/all_to_all | solution.py:533
  105.9 3.5 %states.1 = bf16[16,32,128]{2,1,0:T(8,128)(2,1)} custom-call(bf16[16,64,128]{2,1,0:T(8,128)(2,1)} %all_to_all.16.u_ref), custom_call_target="tpu_custom_call" | custom-call | tf_op jit(solution)/shard_map/states/pallas_call | solution.py:406
  109.4 10.4 %all-to-all-start.2 = ((bf16[16,32,128]{2,1,0:T(8,128)(2,1)}), bf16[16,32,128]{2,1,0:T(8,128)(2,1)S(1)}, u32[]{:S(2)}, u32[]{:S(2)}) async-start(bf16[16,32,128]{2,1,0:T(8,128)(2,1)} %states.1), calls=%async_computation.2 | async-start | bytes 262144 | tf_op jit(solution)/shard_map/all_to_all | solution.py:536
  119.8 11.6 %outputs.1 = (f32[2,512,256]{2,1,0:T(8,128)}, f32[2,512,256]{2,1,0:T(8,128)}, f32[512,256]{1,0:T(8,128)}) custom-call(bf16[512,768]{1,0:T(8,128)(2,1)} %get-tuple-element.17.k_ref.v_ref.q_ref, bf16[512,768]{1,0:T(8,128)(2,1)} %get-tuple-element.17.k_ref.v_ref.q_ref, bf16[512,768]{1,0:T(8,128)(2,1)} %get-tuple-element.17.k_ref.v_ref.q_ref, ...), custom_call_target="tpu_custom_call" | custom-call | flops 4000000000 | bytes 8000000 | tf_op jit(solution)/shard_map/outputs/pallas_call | solution.py:309
  131.4 0.4 all-to-all-done.2.s_ref
  131.8 0.7 copy-done.6
  132.4 4.4 %final.1 = (bf16[128,256]{1,0:T(8,128)(2,1)}, bf16[128,256]{1,0:T(8,128)(2,1)}, bf16[128,256]{1,0:T(8,128)(2,1)}, bf16[128,256]{1,0:T(8,128)(2,1)}) custom-call(f32[2,512,256]{2,1,0:T(8,128)} %get-tuple-element.21.y_ref, f32[2,512,256]{2,1,0:T(8,128)} %get-tuple-element.22.qx_ref, bf16[16,32,128]{2,1,0:T(8,128)(2,1)} %copy-done.6, ...), custom_call_target="tpu_custom_call" | custom-call | tf_op jit(solution)/shard_map/final/pallas_call | solution.py:367
  136.8 2.9 %collective-permute-start.10 = (bf16[128,256]{1,0:T(8,128)(2,1)}, bf16[128,256]{1,0:T(8,128)(2,1)S(1)}, u32[]{:S(2)}, u32[]{:S(2)}) collective-permute-start(bf16[128,256]{1,0:T(8,128)(2,1)} %get-tuple-element.26), channel_id=1, source_target_pairs={{0,32},{32,0},{64,96},{96,64},{128,160},{160,128},{192,224},{224,1... | collective-permute-start | bytes 196616 | tf_op jit(solution)/shard_map/ppermute | solution.py:541
  139.7 5.6 %collective-permute-start.11 = (bf16[128,256]{1,0:T(8,128)(2,1)}, bf16[128,256]{1,0:T(8,128)(2,1)S(1)}, u32[]{:S(2)}, u32[]{:S(2)}) collective-permute-start(bf16[128,256]{1,0:T(8,128)(2,1)} %get-tuple-element.27), channel_id=1, source_target_pairs={{0,1},{1,0},{2,3},{3,2},{4,5},{5,4},{6,7},{7,6},{8,9},{9,8},{10,11... | collective-permute-start | bytes 196616 | tf_op jit(solution)/shard_map/ppermute | solution.py:542
  145.3 2.8 %collective-permute-start.12 = (bf16[128,256]{1,0:T(8,128)(2,1)}, bf16[128,256]{1,0:T(8,128)(2,1)S(1)}, u32[]{:S(2)}, u32[]{:S(2)}) collective-permute-start(bf16[128,256]{1,0:T(8,128)(2,1)} %get-tuple-element.28), channel_id=1, source_target_pairs={{0,33},{1,32},{2,35},{3,34},{4,37},{5,36},{6,39},{7,38},{8,41},{9,... | collective-permute-start | bytes 196616 | tf_op jit(solution)/shard_map/ppermute | solution.py:538
  148.2 0.0 collective-permute-done.11
  148.2 2.9 %collective-permute-done.12 = bf16[128,256]{1,0:T(8,128)(2,1)S(1)} collective-permute-done((bf16[128,256]{1,0:T(8,128)(2,1)}, bf16[128,256]{1,0:T(8,128)(2,1)S(1)}, u32[]{:S(2)}, u32[]{:S(2)}) %collective-permute-start.12) | collective-permute-done | bytes 65568 | tf_op jit(solution)/shard_map/ppermute | solution.py:538
  151.2 0.9 broadcast_select_fusion.7
  152.0 0.7 maximum_bitcast_fusion
  (22 shorter events, 0.1 us)
Async XLA Ops:
  0.0 43.4 %copy-start.9 = (f32[64]{0:T(128)S(1)}, f32[64]{0:T(128)}, u32[]{:S(2)}) copy-start(f32[64]{0:T(128)} %param.19) | copy-start | bytes 772
  0.0 43.4 %copy-start.8 = (f32[2,64]{1,0:T(2,128)S(1)}, f32[2,64]{1,0:T(2,128)}, u32[]{:S(2)}) copy-start(f32[2,64]{1,0:T(2,128)} %param.17) | copy-start | bytes 1540
  0.0 43.4 %copy-start.7 = (f32[2,64]{1,0:T(2,128)S(1)}, f32[2,64]{1,0:T(2,128)}, u32[]{:S(2)}) copy-start(f32[2,64]{1,0:T(2,128)} %param.18) | copy-start | bytes 1540
  2.4 9.7 %collective-permute-start = (bf16[64,1024]{1,0:T(8,128)(2,1)S(1)}, bf16[64,1024]{1,0:T(8,128)(2,1)S(1)}, u32[]{:S(2)}, u32[]{:S(2)}) collective-permute-start(bf16[64,1024]{1,0:T(8,128)(2,1)S(1)} %pad_maximum_fusion.1), channel_id=1, source_target_pairs={{0,1},{1,0},{2,3},{3,2},{4,5},{5,4},{6,7},{7,6},{8,9},{9,8},{10,11... | collective-permute-start | bytes 393224 | tf_op jit(solution)/shard_map/ppermute | solution.py:514
  13.0 55.4 %copy-start = (bf16[128,1024]{1,0:T(8,128)(2,1)}, bf16[128,1024]{1,0:T(8,128)(2,1)S(1)}, u32[]{:S(2)}) copy-start(bf16[128,1024]{1,0:T(8,128)(2,1)S(1)} %maximum_select_fusion.b0) | copy-start | bytes 786436
  13.0 10.4 %collective-permute-start.1 = (bf16[128,1024]{1,0:T(8,128)(2,1)S(1)}, bf16[128,1024]{1,0:T(8,128)(2,1)S(1)}, u32[]{:S(2)}, u32[]{:S(2)}) collective-permute-start(bf16[128,1024]{1,0:T(8,128)(2,1)S(1)} %maximum_select_fusion.b0), channel_id=1, source_target_pairs={{0,2},{1,9},{2,4},{3,11},{4,6},{5,13},{6,0},{7,15},{8,10},{9,17},{... | collective-permute-start | bytes 786440 | tf_op jit(solution)/shard_map/ppermute | solution.py:516
  15.0 10.7 %collective-permute-start.2 = (bf16[128,1024]{1,0:T(8,128)(2,1)S(1)}, bf16[128,1024]{1,0:T(8,128)(2,1)S(1)}, u32[]{:S(2)}, u32[]{:S(2)}) collective-permute-start(bf16[128,1024]{1,0:T(8,128)(2,1)S(1)} %maximum_select_fusion.b0), channel_id=1, source_target_pairs={{0,6},{1,25},{2,0},{3,27},{4,2},{5,29},{6,4},{7,31},{8,14},{9,1},{... | collective-permute-start | bytes 786440 | tf_op jit(solution)/shard_map/ppermute | solution.py:517
  19.6 8.9 %collective-permute-start.3 = (bf16[128,1024]{1,0:T(8,128)(2,1)S(1)}, bf16[128,1024]{1,0:T(8,128)(2,1)S(1)}, u32[]{:S(2)}, u32[]{:S(2)}) collective-permute-start(bf16[128,1024]{1,0:T(8,128)(2,1)S(1)} %maximum_select_fusion.b0), channel_id=1, source_target_pairs={{0,4},{1,17},{2,6},{3,19},{4,0},{5,21},{6,2},{7,23},{8,12},{9,25},... | collective-permute-start | bytes 786440 | tf_op jit(solution)/shard_map/ppermute | solution.py:518
  21.5 19.9 %collective-permute-start.7 = (bf16[128,2048]{1,0:T(8,128)(2,1)}, bf16[128,2048]{1,0:T(8,128)(2,1)}, u32[]{:S(2)}, u32[]{:S(2)}) collective-permute-start(bf16[128,2048]{1,0:T(8,128)(2,1)} %bitcast.t0), channel_id=1, source_target_pairs={{0,32},{32,0},{64,96},{96,64},{128,160},{160,128},{192,224},{224,1... | collective-permute-start | bytes 1572872 | tf_op jit(solution)/shard_map/ppermute | solution.py:519
  23.4 13.6 %copy-start.3 = (bf16[128,1024]{1,0:T(8,128)(2,1)}, bf16[128,1024]{1,0:T(8,128)(2,1)S(1)}, u32[]{:S(2)}) copy-start(bf16[128,1024]{1,0:T(8,128)(2,1)S(1)} %collective-permute-done.1.fm) | copy-start | bytes 786436
  25.7 15.7 %copy-start.4 = (bf16[128,1024]{1,0:T(8,128)(2,1)}, bf16[128,1024]{1,0:T(8,128)(2,1)S(1)}, u32[]{:S(2)}) copy-start(bf16[128,1024]{1,0:T(8,128)(2,1)S(1)} %collective-permute-done.2.fp) | copy-start | bytes 786436
  28.5 12.9 %copy-start.5 = (bf16[128,1024]{1,0:T(8,128)(2,1)}, bf16[128,1024]{1,0:T(8,128)(2,1)S(1)}, u32[]{:S(2)}) copy-start(bf16[128,1024]{1,0:T(8,128)(2,1)S(1)} %collective-permute-done.3.fo) | copy-start | bytes 786436
  28.5 39.8 %collective-permute-start.4 = (bf16[512,1024]{1,0:T(8,128)(2,1)S(1)}, bf16[512,1024]{1,0:T(8,128)(2,1)S(1)}, u32[]{:S(2)}, u32[]{:S(2)}) collective-permute-start(bf16[512,1024]{1,0:T(8,128)(2,1)S(1)} %pad_maximum_fusion), channel_id=1, source_target_pairs={{0,8},{1,3},{2,10},{3,5},{4,12},{5,7},{6,14},{7,1},{8,16},{9,11},{... | collective-permute-start | bytes 3145736 | tf_op jit(solution)/shard_map/ppermute | solution.py:526
  30.5 37.9 %collective-permute-start.5 = (bf16[512,1024]{1,0:T(8,128)(2,1)S(1)}, bf16[512,1024]{1,0:T(8,128)(2,1)S(1)}, u32[]{:S(2)}, u32[]{:S(2)}) collective-permute-start(bf16[512,1024]{1,0:T(8,128)(2,1)S(1)} %pad_maximum_fusion), channel_id=1, source_target_pairs={{0,24},{1,7},{2,26},{3,1},{4,28},{5,3},{6,30},{7,5},{8,0},{9,15},{... | collective-permute-start | bytes 3145736 | tf_op jit(solution)/shard_map/ppermute | solution.py:527
  35.1 33.4 %collective-permute-start.6 = (bf16[512,1024]{1,0:T(8,128)(2,1)S(1)}, bf16[512,1024]{1,0:T(8,128)(2,1)}, u32[]{:S(2)}, u32[]{:S(2)}) collective-permute-start(bf16[512,1024]{1,0:T(8,128)(2,1)S(1)} %pad_maximum_fusion), channel_id=1, source_target_pairs={{0,16},{1,5},{2,18},{3,7},{4,20},{5,1},{6,22},{7,3},{8,24},{9,13},... | collective-permute-start | bytes 3145736 | tf_op jit(solution)/shard_map/ppermute | solution.py:528
  37.0 31.4 %collective-permute-start.8 = (bf16[128,2048]{1,0:T(8,128)(2,1)}, bf16[128,2048]{1,0:T(8,128)(2,1)}, u32[]{:S(2)}, u32[]{:S(2)}) collective-permute-start(bf16[128,2048]{1,0:T(8,128)(2,1)} %bitcast.t0), channel_id=1, source_target_pairs={{0,1},{1,0},{2,3},{3,2},{4,5},{5,4},{6,7},{7,6},{8,9},{9,8},{10,11... | collective-permute-start | bytes 1572872 | tf_op jit(solution)/shard_map/ppermute | solution.py:520
  41.4 27.0 %collective-permute-start.9 = (bf16[128,2048]{1,0:T(8,128)(2,1)}, bf16[128,2048]{1,0:T(8,128)(2,1)}, u32[]{:S(2)}, u32[]{:S(2)}) collective-permute-start(bf16[128,2048]{1,0:T(8,128)(2,1)} %collective-permute-done.7.t1), channel_id=1, source_target_pairs={{0,1},{1,0},{2,3},{3,2},{4,5},{5,4},{6,7},{7,6},{8,9},{9,8},{10,11... | collective-permute-start | bytes 1572872 | tf_op jit(solution)/shard_map/ppermute | solution.py:529
  68.4 1.0 copy-start.1
  68.4 1.3 copy-start.2
  109.4 22.4 %all-to-all-start.2 = ((bf16[16,32,128]{2,1,0:T(8,128)(2,1)}), bf16[16,32,128]{2,1,0:T(8,128)(2,1)S(1)}, u32[]{:S(2)}, u32[]{:S(2)}) async-start(bf16[16,32,128]{2,1,0:T(8,128)(2,1)} %states.1), calls=%async_computation.2 | async-start | bytes 262144 | tf_op jit(solution)/shard_map/all_to_all | solution.py:536
  131.8 0.7 copy-start.6
  136.8 11.4 %collective-permute-start.10 = (bf16[128,256]{1,0:T(8,128)(2,1)}, bf16[128,256]{1,0:T(8,128)(2,1)S(1)}, u32[]{:S(2)}, u32[]{:S(2)}) collective-permute-start(bf16[128,256]{1,0:T(8,128)(2,1)} %get-tuple-element.26), channel_id=1, source_target_pairs={{0,32},{32,0},{64,96},{96,64},{128,160},{160,128},{192,224},{224,1... | collective-permute-start | bytes 196616 | tf_op jit(solution)/shard_map/ppermute | solution.py:541
  139.7 8.5 %collective-permute-start.11 = (bf16[128,256]{1,0:T(8,128)(2,1)}, bf16[128,256]{1,0:T(8,128)(2,1)S(1)}, u32[]{:S(2)}, u32[]{:S(2)}) collective-permute-start(bf16[128,256]{1,0:T(8,128)(2,1)} %get-tuple-element.27), channel_id=1, source_target_pairs={{0,1},{1,0},{2,3},{3,2},{4,5},{5,4},{6,7},{7,6},{8,9},{9,8},{10,11... | collective-permute-start | bytes 196616 | tf_op jit(solution)/shard_map/ppermute | solution.py:542
  145.3 5.8 %collective-permute-start.12 = (bf16[128,256]{1,0:T(8,128)(2,1)}, bf16[128,256]{1,0:T(8,128)(2,1)S(1)}, u32[]{:S(2)}, u32[]{:S(2)}) collective-permute-start(bf16[128,256]{1,0:T(8,128)(2,1)} %get-tuple-element.28), channel_id=1, source_target_pairs={{0,33},{1,32},{2,35},{3,34},{4,37},{5,36},{6,39},{7,38},{8,41},{9,... | collective-permute-start | bytes 196616 | tf_op jit(solution)/shard_map/ppermute | solution.py:538
